TPU v7x, 32 devices: a whole 2x2x4 slice. The times are simulated.
32 devices in a mesh: sp: 16 (over z, y, x), tp: 2 (over core).
Axes of the slice: x: 2, y: 2, z: 4, core: 2. Of those that a mesh axis runs over, the one named last changes fastest.
Arguments:
- hidden_in: bfloat16 [4096, 2048], P('sp'), may hold values from -16 to 16
- query_one: bfloat16 [2048, 512], P(None, 'tp'), may hold values from -0.13258252 to 0.13258252
- query_two: bfloat16 [2048, 512], P(None, 'tp'), may hold values from -0.13258252 to 0.13258252
- key_one: bfloat16 [2048, 512], P(None, 'tp'), may hold values from -0.13258252 to 0.13258252
- key_two: bfloat16 [2048, 512], P(None, 'tp'), may hold values from -0.13258252 to 0.13258252
- value_proj: bfloat16 [2048, 1024], P(None, 'tp'), may hold values from -0.125 to 0.125
- lambdas: float32 [8], P('tp'), may hold values from 0.3 to 0.8
- norm_gain: float32 [128], replicated, may hold values from 0.1 to 1.9
- out_proj: bfloat16 [1024, 2048], P('tp'), may hold values from -0.1875 to 0.1875
Outputs:
- attended: bfloat16 [4096, 2048], P('sp')
All inputs are finite; a program needn't handle non-finite values.
Results may differ from a plain program's by a relative error of at most 0.015.
Values may be sent and summed in bfloat16 or wider, within the bound.
A program may use at most 64 MiB of HBM per device.

v0:
```python
import math

import jax
import jax.numpy as jnp
from jax import lax
from jax.experimental import pallas as pl
from jax.experimental.pallas import tpu as pltpu
from jax.sharding import PartitionSpec as P

epsilon = 1e-06
masked_score = -1e30


def shards(
    hidden_in, query_one, query_two, key_one, key_two, value_proj, lambdas, norm_gain, out_proj
):
    heads_dev = lambdas.shape[0]
    head_qk = query_one.shape[1] // heads_dev
    head_v = value_proj.shape[1] // heads_dev
    width_q = heads_dev * head_qk
    score_scale = 1.75 * head_qk ** (-0.5)
    joined = jnp.concatenate((query_one, query_two, key_one, key_two, value_proj), axis=1)
    projected = jnp.dot(hidden_in, joined, preferred_element_type=jnp.float32).astype(jnp.bfloat16)
    tok_rows = projected.shape[0]
    key_values = projected[:, 2 * width_q :]
    my_index = lax.axis_index("sp")
    offset = my_index * tok_rows
    query_sets = (projected[:, : 2 * width_q],)
    position_sets = (offset + jnp.arange(tok_rows, dtype=jnp.int32),)
    groups = []
    for query_rows, positions in zip(query_sets, position_sets):
        group_rows = query_rows.shape[0]
        query_a = query_rows[:, :width_q].reshape(group_rows, heads_dev, head_qk)
        query_b = query_rows[:, width_q:].reshape(group_rows, heads_dev, head_qk)
        groups.append((query_a, query_b, positions, positions[group_rows - 1]))

    def one_map(queries, keys, value_rows, allowed, running_max, running_sum, accum):
        scores = (
            jnp.einsum("qhd,khd->hqk", queries, keys, preferred_element_type=jnp.float32)
            * score_scale
        )
        scores = jnp.where(allowed[None], scores, masked_score)
        new_max = jnp.maximum(running_max, jnp.max(scores, axis=-1))
        rescale = jnp.exp(running_max - new_max)
        weights = jnp.where(allowed[None], jnp.exp(scores - new_max[..., None]), 0.0)
        new_sum = running_sum * rescale + jnp.sum(weights, axis=-1)
        added = jnp.einsum(
            "hqk,khe->hqe",
            weights.astype(jnp.bfloat16),
            value_rows,
            preferred_element_type=jnp.float32,
        )
        return (new_max, new_sum, accum * rescale[..., None] + added)

    def absorb(group_state, group, kblock, kstart):
        query_a, query_b, positions, last_pos = group
        block_rows = kblock.shape[0]
        k_pos = kstart + jnp.arange(block_rows, dtype=jnp.int32)
        allowed = k_pos[None, :] <= positions[:, None]
        keys_a = kblock[:, :width_q].reshape(block_rows, heads_dev, head_qk)
        keys_b = kblock[:, width_q : 2 * width_q].reshape(block_rows, heads_dev, head_qk)
        value_rows = kblock[:, 2 * width_q :].reshape(block_rows, heads_dev, head_v)
        first_map = one_map(query_a, keys_a, value_rows, allowed, *group_state[:3])
        second_map = one_map(query_b, keys_b, value_rows, allowed, *group_state[3:])
        return first_map + second_map

    group = groups[0]
    group_rows = group[0].shape[0]
    start_max = jnp.full((heads_dev, group_rows), masked_score, jnp.float32)
    start_sum = jnp.zeros((heads_dev, group_rows), jnp.float32)
    start_acc = jnp.zeros((heads_dev, group_rows, head_v), jnp.float32)
    initial_list = [(start_max, start_sum, start_acc, start_max, start_sum, start_acc)]
    initial = tuple(initial_list)
    softmax_state = initial
    kv_piece = lax.all_gather(key_values, "sp", axis=0, tiled=True)
    piece_rows = kv_piece.shape[0]
    block_rows = math.gcd(piece_rows, 512)
    block_count = piece_rows // block_rows
    stacked = kv_piece.reshape(block_count, block_rows, kv_piece.shape[1])

    def absorb_step(carried, blocks_in):
        kblock, block_index = blocks_in
        kstart = block_index * block_rows
        renewed = []
        for group, group_state in zip(groups, carried):
            renewed.append(
                lax.cond(
                    kstart <= group[3],
                    lambda inner, group=group: absorb(inner, group, kblock, kstart),
                    lambda inner: inner,
                    group_state,
                )
            )
        return (tuple(renewed), None)

    softmax_state, _ = lax.scan(
        absorb_step, softmax_state, (stacked, jnp.arange(block_count, dtype=jnp.int32))
    )
    normed_sets = []
    for group_state in softmax_state:
        out_a = group_state[2] / group_state[1][..., None]
        out_b = group_state[5] / group_state[4][..., None]
        mixed_out = out_a - lambdas[:, None, None] * out_b
        scale_rows = lax.rsqrt(jnp.mean(mixed_out * mixed_out, axis=-1, keepdims=True) + epsilon)
        normed = (mixed_out * scale_rows * norm_gain).astype(jnp.bfloat16)
        group_rows = normed.shape[1]
        normed_sets.append(jnp.transpose(normed, (1, 0, 2)).reshape(group_rows, heads_dev * head_v))
    normed_all = normed_sets[0]
    partial_value = jnp.dot(normed_all, out_proj, preferred_element_type=jnp.float32)
    result = lax.psum(partial_value.astype(jnp.bfloat16), "tp")
    return result


MESH = pl.DeviceIdType.MESH
PLANE = 4


def fused_kernel(
    groups,
    score_scale,
    hidden_hbm,
    q1_hbm,
    q2_hbm,
    k1_hbm,
    k2_hbm,
    v_hbm,
    lam_ref,
    gain_ref,
    wo_hbm,
    out_ref,
    hid,
    wq1,
    wq2,
    wk1,
    wk2,
    wv,
    wo,
    kv_out,
    q_out,
    kv_all,
    q_all,
    n_out,
    n_all,
    max_all,
    sum_all,
    acc_all,
    load_sem,
    wo_send,
    wo_recv,
    kv_send,
    kv_recv,
    q_send,
    q_recv,
    x_send,
    x_recv,
    y_send,
    y_recv,
    f_send,
    f_recv,
    n_send,
    n_recv,
    r_send,
    r_recv,
):
    me = lax.axis_index("sp")
    core = lax.axis_index("tp")
    plane = me // PLANE
    spot = lax.rem(me, PLANE)
    x_spot = spot + 1 - 2 * lax.rem(spot, 2)
    y_spot = spot + 2 - 4 * (spot // 2)
    rows = hid.shape[0]
    qk = q1_hbm.shape[1] // groups
    width = 2 * qk

    def load(index, src, dst):
        return pltpu.make_async_copy(src, dst, load_sem.at[index])

    loads = [
        load(0, hidden_hbm, hid),
        load(1, k1_hbm, wk1),
        load(2, k2_hbm, wk2),
        load(3, v_hbm, wv),
        load(4, q1_hbm, wq1),
        load(5, q2_hbm, wq2),
        load(6, wo_hbm, wo.at[core]),
    ]
    barrier = pltpu.get_barrier_semaphore()

    def greet(index, tp_index):
        pl.semaphore_signal(
            barrier, inc=1, device_id=(index, tp_index), device_id_type=MESH
        )

    for step in range(1, groups):
        other = lax.rem(plane + step, groups) * PLANE + spot
        greet(other, core)
    greet(me, 1 - core)
    greet(plane * PLANE + x_spot, core)
    greet(plane * PLANE + y_spot, core)

    for item in loads:
        item.start()

    def send(src, dst, send_sem, recv_sem, index, tp_index):
        return pltpu.make_async_remote_copy(
            src_ref=src,
            dst_ref=dst,
            send_sem=send_sem,
            recv_sem=recv_sem,
            device_id=(index, tp_index),
            device_id_type=MESH,
        )

    upper = plane >= groups // 2
    mirrored = jnp.where(upper, groups - 1 - plane, plane)

    def from_plane(step):
        if step == 0:
            return plane
        near = jnp.where(step - 1 < mirrored, step - 1, step)
        return jnp.where(upper, groups - 1 - near, near)

    loads[0].wait()
    pending = []

    def project(weight_ref):
        return jnp.dot(hid[...], weight_ref[...], preferred_element_type=jnp.float32)

    loads[1].wait()
    first = project(wk1).astype(jnp.bfloat16)
    loads[2].wait()
    second = project(wk2).astype(jnp.bfloat16)
    for head in range(groups):
        cut = slice(head * qk, (head + 1) * qk)
        kv_out[head, :, :width] = jnp.concatenate((first[:, cut], second[:, cut]), axis=1)
    loads[3].wait()
    head_v = v_hbm.shape[1] // groups
    for head in range(groups):
        cut = slice(head * head_v, (head + 1) * head_v)
        kv_out[head, :, width:] = jnp.dot(
            hid[...], wv[:, cut], preferred_element_type=jnp.float32
        ).astype(jnp.bfloat16)
    kv_all[me] = kv_out[plane]
    loads[4].wait()
    first = (project(wq1) * score_scale).astype(jnp.bfloat16)
    loads[5].wait()
    second = (project(wq2) * score_scale).astype(jnp.bfloat16)
    for head in range(groups):
        cut = slice(head * qk, (head + 1) * qk)
        q_out[head] = jnp.concatenate((first[:, cut], second[:, cut]), axis=1)
    q_all[plane] = q_out[plane]
    pl.semaphore_wait(barrier, groups - 1 + 3)

    def kv_copy(step):
        target = from_plane(step)
        return send(
            kv_out.at[target],
            kv_all.at[me],
            kv_send.at[step],
            kv_recv.at[plane],
            target * PLANE + spot,
            core,
        )

    def q_copy(step):
        target = from_plane(step)
        return send(
            q_out.at[target],
            q_all.at[plane],
            q_send.at[step],
            q_recv.at[plane],
            target * PLANE + spot,
            core,
        )

    def spread(step):
        block = from_plane(step) * PLANE + spot
        for sems, where in (((x_send, x_recv), x_spot), ((y_send, y_recv), y_spot)):
            copy = send(
                kv_all.at[block],
                kv_all.at[block],
                sems[0].at[step],
                sems[1].at[step],
                plane * PLANE + where,
                core,
            )
            copy.start()
            pending.append(copy)

    def arrived(recv_sem, block):
        pltpu.make_async_copy(kv_all.at[block], kv_all.at[block], recv_sem).wait()

    half = rows // 2

    def relay(step):
        x_block = from_plane(step) * PLANE + x_spot
        y_block = from_plane(step) * PLANE + y_spot
        for part, block, sem, where in (
            (0, x_block, x_recv, y_spot),
            (1, y_block, y_recv, x_spot),
        ):
            arrived(sem.at[step], block)
            piece = kv_all.at[block, pl.ds(part * half, half), :]
            copy = send(
                piece,
                piece,
                f_send.at[step, part],
                f_recv.at[step, part],
                plane * PLANE + where,
                core,
            )
            copy.start()
            pending.append(copy)

    kv_copy(1).start()
    spread(0)
    for step in range(2, groups):
        kv_copy(step).start()
        q_copy(step - 1).start()
    q_copy(groups - 1).start()
    loads[6].wait()
    wo_copy = send(wo.at[core], wo.at[core], wo_send, wo_recv, me, 1 - core)
    wo_copy.start()

    def forward_arrival(step):
        arrived(kv_recv.at[from_plane(step)], from_plane(step) * PLANE + spot)
        spread(step)

    def stage_ready(step):
        far = from_plane(step) * PLANE + (PLANE - 1 - spot)
        for part in range(2):
            piece = kv_all.at[far, pl.ds(part * half, half), :]
            pltpu.make_async_copy(piece, piece, f_recv.at[step, part]).wait()
        if step > 0:
            slot = q_all.at[from_plane(step)]
            pltpu.make_async_copy(slot, slot, q_recv.at[from_plane(step)]).wait()

    tile = ROW_TILE
    tiles = rows // tile
    chunk = PLANE * rows
    lane = lax.broadcasted_iota(jnp.int32, (tile, width), 1)
    lam = lam_ref[plane]
    gain = gain_ref[...]

    def pair_tile(group, key_group, part, diagonal):
        begin = pl.multiple_of(part * tile, tile)
        queries = q_all[group, pl.ds(begin, tile), :]
        zero = jnp.zeros_like(queries)
        both = jnp.concatenate(
            (jnp.where(lane < qk, queries, zero), jnp.where(lane >= qk, queries, zero)), axis=0
        )
        block = kv_all[pl.ds(key_group * PLANE, PLANE)].reshape(chunk, width + head_v)
        scores = lax.dot_general(
            both,
            block[:, :width],
            (((1,), (1,)), ((), ())),
            preferred_element_type=jnp.float32,
        )
        if diagonal:
            q_pos = spot * rows + begin + lax.rem(
                lax.broadcasted_iota(jnp.int32, (2 * tile, chunk), 0), tile
            )
            k_pos = lax.broadcasted_iota(jnp.int32, (2 * tile, chunk), 1)
            scores = jnp.where(k_pos <= q_pos, scores, masked_score)
        new_max = jnp.max(scores, axis=-1, keepdims=True)
        if not diagonal:
            running_max = max_all[group, part]
            new_max = jnp.maximum(running_max, new_max)
            rescale = jnp.exp2(running_max - new_max)
        weights = jnp.exp2(scores - new_max)
        new_sum = jnp.sum(weights, axis=-1, keepdims=True)
        accum = jnp.dot(
            weights.astype(jnp.bfloat16),
            block[:, width:],
            preferred_element_type=jnp.float32,
        )
        if not diagonal:
            new_sum = sum_all[group, part] * rescale + new_sum
            accum = acc_all[group, part] * rescale + accum
        max_all[group, part] = new_max
        sum_all[group, part] = new_sum
        acc_all[group, part] = accum

    def pair(group, key_group, diagonal):
        lax.fori_loop(
            0, tiles, lambda t, c: (pair_tile(group, key_group, t, diagonal), c)[1], 0
        )

    def meet(step, earlier):
        one, other = from_plane(step), from_plane(earlier)
        pair(jnp.maximum(one, other), jnp.minimum(one, other), False)

    def normed_copy(group):
        return send(
            n_out.at[group],
            n_all.at[core, plane],
            n_send.at[group],
            n_recv.at[plane],
            group * PLANE + spot,
            core,
        )

    def partner_copy(head):
        slot = n_all.at[core, head]
        return send(slot, slot, r_send.at[head], r_recv.at[head], me, 1 - core)

    def finish(group):
        def finish_tile(part, _):
            begin = pl.multiple_of(part * tile, tile)
            heads_out = acc_all[group, part] / sum_all[group, part]
            mixed = heads_out[:tile] - lam * heads_out[tile:]
            scale_rows = lax.rsqrt(jnp.mean(mixed * mixed, axis=-1, keepdims=True) + epsilon)
            normed = (mixed * scale_rows * gain).astype(jnp.bfloat16)
            n_out[group, pl.ds(begin, tile), :] = normed
            return 0

        lax.fori_loop(0, tiles, finish_tile, 0)

    def stage(step):
        stage_ready(step)
        pair(from_plane(step), from_plane(step), True)
        if step + 1 < groups:
            for earlier in range(step):
                meet(step, earlier)
        else:
            for earlier in list(range(1, step)) + [0]:
                meet(step, earlier)
                finish(from_plane(earlier))
                if earlier == 0:
                    n_all[core, plane] = n_out[plane]
                    partner_copy(plane).start()
                else:
                    normed_copy(from_plane(earlier)).start()

    for step in range(1, groups):
        forward_arrival(step)
        relay(step - 1)
        if step >= 2:
            stage(step - 2)
    relay(groups - 1)
    stage(groups - 2)
    stage(groups - 1)
    finish(from_plane(groups - 1))
    normed_copy(from_plane(groups - 1)).start()

    for step in range(1, groups):
        head = from_plane(step)
        slot = n_all.at[core, head]
        pltpu.make_async_copy(slot, slot, n_recv.at[head]).wait()
        partner_copy(head).start()
    wo_copy.wait_send()

    def out_tiles(tp_index, first_part):
        normed = jnp.concatenate([n_all[tp_index, head] for head in range(groups)], axis=1)

        def out_tile(index, _):
            columns = pl.ds(pl.multiple_of(index * OUT_TILE, OUT_TILE), OUT_TILE)
            part = jnp.dot(normed, wo[tp_index, :, columns], preferred_element_type=jnp.float32)
            part = part.astype(jnp.bfloat16)
            if not first_part:
                part = (part.astype(jnp.float32) + out_ref[:, columns].astype(jnp.float32)).astype(
                    jnp.bfloat16
                )
            out_ref[:, columns] = part
            return 0

        lax.fori_loop(0, out_ref.shape[1] // OUT_TILE, out_tile, 0)

    out_tiles(core, True)
    pltpu.make_async_copy(wo.at[1 - core], wo.at[1 - core], wo_recv).wait()
    for head in range(groups):
        slot = n_all.at[1 - core, head]
        pltpu.make_async_copy(slot, slot, r_recv.at[head]).wait()
    out_tiles(1 - core, False)

    for copy in pending:
        copy.wait_send()
    for step in range(1, groups):
        kv_copy(step).wait_send()
        q_copy(step).wait_send()
        normed_copy(from_plane(step)).wait_send()
    for head in range(groups):
        partner_copy(head).wait_send()


ROW_TILE = 256
OUT_TILE = 1024


def fused_shards(
    hidden_in, query_one, query_two, key_one, key_two, value_proj, lambdas, norm_gain, out_proj
):
    groups = lambdas.shape[0]
    rows, depth = hidden_in.shape
    head_qk = query_one.shape[1] // groups
    head_v = value_proj.shape[1] // groups
    width = 2 * head_qk
    blocks = groups * PLANE
    columns = out_proj.shape[1]
    score_scale = 1.75 * head_qk ** (-0.5) * math.log2(math.e)
    bf16 = jnp.bfloat16
    dma = pltpu.SemaphoreType.DMA
    hbm = pl.BlockSpec(memory_space=pl.ANY)
    vmem = pl.BlockSpec(memory_space=pltpu.VMEM)
    smem = pl.BlockSpec(memory_space=pltpu.SMEM)

    def body(*refs):
        fused_kernel(groups, score_scale, *refs)

    return pl.pallas_call(
        body,
        name="fused_attention",
        out_shape=jax.ShapeDtypeStruct((rows, columns), bf16),
        in_specs=[hbm] * 6 + [smem, vmem, hbm],
        out_specs=vmem,
        scratch_shapes=[
            pltpu.VMEM(hidden_in.shape, bf16),
            pltpu.VMEM(query_one.shape, bf16),
            pltpu.VMEM(query_two.shape, bf16),
            pltpu.VMEM(key_one.shape, bf16),
            pltpu.VMEM(key_two.shape, bf16),
            pltpu.VMEM(value_proj.shape, bf16),
            pltpu.VMEM((2,) + out_proj.shape, bf16),
            pltpu.VMEM((groups, rows, width + head_v), bf16),
            pltpu.VMEM((groups, rows, width), bf16),
            pltpu.VMEM((blocks, rows, width + head_v), bf16),
            pltpu.VMEM((groups, rows, width), bf16),
            pltpu.VMEM((groups, rows, head_v), bf16),
            pltpu.VMEM((2, groups, rows, head_v), bf16),
            pltpu.VMEM((groups, rows // ROW_TILE, 2 * ROW_TILE, 1), jnp.float32),
            pltpu.VMEM((groups, rows // ROW_TILE, 2 * ROW_TILE, 1), jnp.float32),
            pltpu.VMEM((groups, rows // ROW_TILE, 2 * ROW_TILE, head_v), jnp.float32),
            dma((7,)),
            dma,
            dma,
        ]
        + [dma((groups,))] * 8
        + [dma((groups, 2))] * 2
        + [dma((groups,))] * 4,
        compiler_params=pltpu.CompilerParams(
            collective_id=0, has_side_effects=True, vmem_limit_bytes=60 * 1024 * 1024
        ),
    )(
        hidden_in,
        query_one,
        query_two,
        key_one,
        key_two,
        value_proj,
        lambdas,
        norm_gain.reshape(1, head_v),
        out_proj,
    )


def solution(mesh):
    placed = (
        P("sp", None),
        P(None, "tp"),
        P(None, "tp"),
        P(None, "tp"),
        P(None, "tp"),
        P(None, "tp"),
        P("tp"),
        P(),
        P("tp", None),
    )

    def body(*args):
        groups = args[6].shape[0]
        split = groups * PLANE == mesh.shape["sp"] and mesh.shape["tp"] == 2
        return (fused_shards if split else shards)(*args)

    return jax.shard_map(
        body, mesh=mesh, in_specs=placed, out_specs=P("sp", None), check_vma=False
    )
```

profile of v0, /device:TPU:0, one launch (start us, length us, event | category | flops | bytes accessed | tf_op | source)
XLA Modules:
  0.0 55.5 jit_solution(9074404866692884829)
XLA Ops:
  0.0 53.2 %fused_attention.1 = bf16[256,2048]{1,0:T(8,128)(2,1)} custom-call(bf16[256,2048]{1,0:T(8,128)(2,1)} %refs_0_.1, bf16[2048,256]{1,0:T(8,128)(2,1)} %refs_1_.1, bf16[2048,256]{1,0:T(8,128)(2,1)} %refs_2_.1, bf16[2048,256]{1,0:T(8,128)(2,1)} %refs_3_.1, bf16[2048,256]{1,0:T(8,128)(2,1)} %refs_4_.1, bf16[2048,512]{1,0:T(8,128)(2,1)} %refs_5_.1, f32[4]{0:T(128)} %refs_6_.1, ...), custom_call_target="tpu_custom_call" | custom-call | tf_op jit(solution)/shard_map/fused_attention/pallas_call | solution.py:510
  53.2 2.3 %copy.11 = bf16[256,2048]{1,0:T(8,128)(2,1)} copy(bf16[256,2048]{1,0:T(8,128)(2,1)} %fused_attention.1) | data formatting | bytes 2097152
where the time goes:
time: 55.7 us; the launch traced here: 55.5 us
  Pallas kernels  53.2 us (96%)
  local copies, waits for them, and re-layouts  2.3 us (4%)
    pallas_call x1, Pallas kernels, fused_shards(): pl.pallas_call(body, name='fused_attention', out_shape=jax.ShapeDtypeStru...  53.2 us
    unnamed x1, local copies, waits for them, and re-layouts  2.3 us

commit v1 on v0

v1 whole, which is shorter than its diff:
```python
import math

import jax
import jax.numpy as jnp
from jax import lax
from jax.experimental import pallas as pl
from jax.experimental.pallas import tpu as pltpu
from jax.sharding import PartitionSpec as P

epsilon = 1e-06
masked_score = -1e30


def shards(
    hidden_in, query_one, query_two, key_one, key_two, value_proj, lambdas, norm_gain, out_proj
):
    heads_dev = lambdas.shape[0]
    head_qk = query_one.shape[1] // heads_dev
    head_v = value_proj.shape[1] // heads_dev
    width_q = heads_dev * head_qk
    score_scale = 1.75 * head_qk ** (-0.5)
    joined = jnp.concatenate((query_one, query_two, key_one, key_two, value_proj), axis=1)
    projected = jnp.dot(hidden_in, joined, preferred_element_type=jnp.float32).astype(jnp.bfloat16)
    tok_rows = projected.shape[0]
    key_values = projected[:, 2 * width_q :]
    my_index = lax.axis_index("sp")
    offset = my_index * tok_rows
    query_sets = (projected[:, : 2 * width_q],)
    position_sets = (offset + jnp.arange(tok_rows, dtype=jnp.int32),)
    groups = []
    for query_rows, positions in zip(query_sets, position_sets):
        group_rows = query_rows.shape[0]
        query_a = query_rows[:, :width_q].reshape(group_rows, heads_dev, head_qk)
        query_b = query_rows[:, width_q:].reshape(group_rows, heads_dev, head_qk)
        groups.append((query_a, query_b, positions, positions[group_rows - 1]))

    def one_map(queries, keys, value_rows, allowed, running_max, running_sum, accum):
        scores = (
            jnp.einsum("qhd,khd->hqk", queries, keys, preferred_element_type=jnp.float32)
            * score_scale
        )
        scores = jnp.where(allowed[None], scores, masked_score)
        new_max = jnp.maximum(running_max, jnp.max(scores, axis=-1))
        rescale = jnp.exp(running_max - new_max)
        weights = jnp.where(allowed[None], jnp.exp(scores - new_max[..., None]), 0.0)
        new_sum = running_sum * rescale + jnp.sum(weights, axis=-1)
        added = jnp.einsum(
            "hqk,khe->hqe",
            weights.astype(jnp.bfloat16),
            value_rows,
            preferred_element_type=jnp.float32,
        )
        return (new_max, new_sum, accum * rescale[..., None] + added)

    def absorb(group_state, group, kblock, kstart):
        query_a, query_b, positions, last_pos = group
        block_rows = kblock.shape[0]
        k_pos = kstart + jnp.arange(block_rows, dtype=jnp.int32)
        allowed = k_pos[None, :] <= positions[:, None]
        keys_a = kblock[:, :width_q].reshape(block_rows, heads_dev, head_qk)
        keys_b = kblock[:, width_q : 2 * width_q].reshape(block_rows, heads_dev, head_qk)
        value_rows = kblock[:, 2 * width_q :].reshape(block_rows, heads_dev, head_v)
        first_map = one_map(query_a, keys_a, value_rows, allowed, *group_state[:3])
        second_map = one_map(query_b, keys_b, value_rows, allowed, *group_state[3:])
        return first_map + second_map

    group = groups[0]
    group_rows = group[0].shape[0]
    start_max = jnp.full((heads_dev, group_rows), masked_score, jnp.float32)
    start_sum = jnp.zeros((heads_dev, group_rows), jnp.float32)
    start_acc = jnp.zeros((heads_dev, group_rows, head_v), jnp.float32)
    initial_list = [(start_max, start_sum, start_acc, start_max, start_sum, start_acc)]
    initial = tuple(initial_list)
    softmax_state = initial
    kv_piece = lax.all_gather(key_values, "sp", axis=0, tiled=True)
    piece_rows = kv_piece.shape[0]
    block_rows = math.gcd(piece_rows, 512)
    block_count = piece_rows // block_rows
    stacked = kv_piece.reshape(block_count, block_rows, kv_piece.shape[1])

    def absorb_step(carried, blocks_in):
        kblock, block_index = blocks_in
        kstart = block_index * block_rows
        renewed = []
        for group, group_state in zip(groups, carried):
            renewed.append(
                lax.cond(
                    kstart <= group[3],
                    lambda inner, group=group: absorb(inner, group, kblock, kstart),
                    lambda inner: inner,
                    group_state,
                )
            )
        return (tuple(renewed), None)

    softmax_state, _ = lax.scan(
        absorb_step, softmax_state, (stacked, jnp.arange(block_count, dtype=jnp.int32))
    )
    normed_sets = []
    for group_state in softmax_state:
        out_a = group_state[2] / group_state[1][..., None]
        out_b = group_state[5] / group_state[4][..., None]
        mixed_out = out_a - lambdas[:, None, None] * out_b
        scale_rows = lax.rsqrt(jnp.mean(mixed_out * mixed_out, axis=-1, keepdims=True) + epsilon)
        normed = (mixed_out * scale_rows * norm_gain).astype(jnp.bfloat16)
        group_rows = normed.shape[1]
        normed_sets.append(jnp.transpose(normed, (1, 0, 2)).reshape(group_rows, heads_dev * head_v))
    normed_all = normed_sets[0]
    partial_value = jnp.dot(normed_all, out_proj, preferred_element_type=jnp.float32)
    result = lax.psum(partial_value.astype(jnp.bfloat16), "tp")
    return result


MESH = pl.DeviceIdType.MESH
PLANE = 4
ROW_TILE = 256
OUT_TILE = 1024


def fused_kernel(
    groups,
    score_scale,
    hidden_hbm,
    q1_hbm,
    q2_hbm,
    k1_hbm,
    k2_hbm,
    v_hbm,
    lam_hbm,
    gain_hbm,
    wo_hbm,
    out_ref,
    hid,
    wq1,
    wq2,
    wk1,
    wk2,
    wv,
    wo,
    lam_ref,
    gain_ref,
    k_out,
    v_out,
    q_out,
    k_all,
    v_all,
    q_all,
    n_out,
    n_all,
    max_all,
    sum_all,
    acc_all,
    load_sem,
    wo_send,
    wo_recv,
    zk_send,
    zk_recv,
    zv_send,
    zv_recv,
    q_send,
    q_recv,
    xk_send,
    xk_recv,
    xv_send,
    xv_recv,
    yk_send,
    yk_recv,
    yv_send,
    yv_recv,
    fk_send,
    fk_recv,
    fv_send,
    fv_recv,
    n_send,
    n_recv,
    r_send,
    r_recv,
):
    scope = jax.named_scope
    me = lax.axis_index("sp")
    core = lax.axis_index("tp")
    plane = me // PLANE
    spot = lax.rem(me, PLANE)
    x_spot = spot + 1 - 2 * lax.rem(spot, 2)
    y_spot = spot + 2 - 4 * (spot // 2)
    rows = hid.shape[0]
    qk = q1_hbm.shape[1] // groups
    width = 2 * qk
    head_v = v_hbm.shape[1] // groups

    def load(index, src, dst):
        return pltpu.make_async_copy(src, dst, load_sem.at[index])

    loads = [
        load(0, hidden_hbm, hid),
        load(1, k1_hbm, wk1),
        load(2, k2_hbm, wk2),
        load(3, v_hbm, wv),
        load(4, q1_hbm, wq1),
        load(5, q2_hbm, wq2),
        load(6, wo_hbm, wo.at[core]),
        load(7, lam_hbm, lam_ref),
        load(8, gain_hbm, gain_ref),
    ]
    for item in loads:
        item.start()
    barrier = pltpu.get_barrier_semaphore()

    def greet(index, tp_index):
        pl.semaphore_signal(barrier, inc=1, device_id=(index, tp_index), device_id_type=MESH)

    for step in range(1, groups):
        other = lax.rem(plane + step, groups) * PLANE + spot
        greet(other, core)
    greet(me, 1 - core)
    greet(plane * PLANE + x_spot, core)
    greet(plane * PLANE + y_spot, core)

    pending = []

    def send(src, dst, send_sem, recv_sem, index, tp_index):
        return pltpu.make_async_remote_copy(
            src_ref=src,
            dst_ref=dst,
            send_sem=send_sem,
            recv_sem=recv_sem,
            device_id=(index, tp_index),
            device_id_type=MESH,
        )

    def begin(*args):
        copy = send(*args)
        copy.start()
        pending.append(copy)

    def arrived(ref, recv_sem):
        pltpu.make_async_copy(ref, ref, recv_sem).wait()

    upper = plane >= groups // 2
    mirrored = jnp.where(upper, groups - 1 - plane, plane)

    def from_plane(step):
        if step == 0:
            return plane
        near = jnp.where(step - 1 < mirrored, step - 1, step)
        return jnp.where(upper, groups - 1 - near, near)

    def project(weight_ref):
        return jnp.dot(hid[...], weight_ref[...], preferred_element_type=jnp.float32)

    def joined(first, second, store):
        for head in range(groups):
            cut = slice(head * qk, (head + 1) * qk)
            store(head, jnp.concatenate((first[:, cut], second[:, cut]), axis=1))

    outer = jnp.logical_or(plane == 0, plane == groups - 1)
    inner = jnp.logical_not(outer)

    def z_copy(kind, step):
        target = from_plane(step)
        out, full, sems, recvs = {
            "k": (k_out, k_all.at[me], zk_send, zk_recv),
            "v": (v_out, v_all.at[me], zv_send, zv_recv),
            "q": (q_out, q_all.at[plane], q_send, q_recv),
        }[kind]
        return send(
            out.at[target],
            full,
            sems.at[step],
            recvs.at[plane],
            target * PLANE + spot,
            core,
        )

    def z_start(*items):
        for kind, step in items:
            z_copy(kind, step).start()

    def z_done(*items):
        for kind, step in items:
            z_copy(kind, step).wait_send()

    far = [step for step in range(2, groups)]

    def gate(index):
        with scope(f"gate#{index}"):

            @pl.when(outer)
            def _():
                z_done(("v", index))
                if index < groups - 1:
                    z_start(("k", index + 1), ("v", index + 1))
                else:
                    z_start(*(("q", step) for step in far))

            if index < groups - 1:

                @pl.when(inner)
                def _():
                    z_done(("v", index + 1))
                    if index + 1 < groups - 1:
                        z_start(("k", index + 2), ("v", index + 2))
                    else:
                        z_start(*(("q", step) for step in far))

    def x_block(step):
        return from_plane(step) * PLANE + x_spot

    def y_block(step):
        return from_plane(step) * PLANE + y_spot

    def spread_k(step):
        slot = k_all.at[from_plane(step) * PLANE + spot]
        begin(slot, slot, xk_send.at[step], xk_recv.at[step], plane * PLANE + x_spot, core)
        begin(slot, slot, yk_send.at[step], yk_recv.at[step], plane * PLANE + y_spot, core)

    def spread_v(step):
        slot = v_all.at[from_plane(step) * PLANE + spot]
        begin(slot, slot, yv_send.at[step], yv_recv.at[step], plane * PLANE + y_spot, core)
        begin(slot, slot, xv_send.at[step], xv_recv.at[step], plane * PLANE + x_spot, core)

    def forward(step):
        source = from_plane(step)
        with scope(f"zk#s={step}"):
            arrived(k_all.at[source * PLANE + spot], zk_recv.at[source])
        spread_k(step)
        with scope(f"zv#s={step}"):
            arrived(v_all.at[source * PLANE + spot], zv_recv.at[source])
        spread_v(step)

    def relay(step):
        with scope(f"rk#s={step}"):
            slot = k_all.at[x_block(step)]
            arrived(slot, xk_recv.at[step])
        begin(slot, slot, fk_send.at[step], fk_recv.at[step], plane * PLANE + y_spot, core)
        with scope(f"rv#s={step}"):
            slot = v_all.at[y_block(step)]
            arrived(slot, yv_recv.at[step])
        begin(slot, slot, fv_send.at[step], fv_recv.at[step], plane * PLANE + x_spot, core)

    def ready(step):
        far = from_plane(step) * PLANE + (PLANE - 1 - spot)
        with scope(f"ready#s={step}"):
            arrived(v_all.at[x_block(step)], xv_recv.at[step])
            arrived(k_all.at[y_block(step)], yk_recv.at[step])
            arrived(k_all.at[far], fk_recv.at[step])
            arrived(v_all.at[far], fv_recv.at[step])

    def ready_q(step):
        with scope(f"q#s={step}"):
            slot = q_all.at[from_plane(step)]
            arrived(slot, q_recv.at[from_plane(step)])

    with scope("w_hid"):
        loads[0].wait()
    with scope("w_k"):
        loads[1].wait()
        loads[2].wait()
    with scope("p_k"):
        first = project(wk1).astype(jnp.bfloat16)
        second = project(wk2).astype(jnp.bfloat16)

        def put_k(head, value):
            k_out[head] = value

        joined(first, second, put_k)
        k_all[me] = k_out[plane]
    with scope("barrier"):
        pl.semaphore_wait(barrier, groups - 1 + 3)
    z_start(("k", 1))
    pl.when(inner)(lambda: z_start(("k", 2)))
    spread_k(0)
    with scope("w_v"):
        loads[3].wait()
    with scope("p_v"):
        value = project(wv).astype(jnp.bfloat16)
        for head in range(groups):
            v_out[head] = value[:, head * head_v : (head + 1) * head_v]
        v_all[me] = v_out[plane]
    z_start(("v", 1))
    pl.when(inner)(lambda: z_start(("v", 2)))
    spread_v(0)
    with scope("w_q"):
        loads[4].wait()
        loads[5].wait()
    with scope("p_q"):
        first = (project(wq1) * score_scale).astype(jnp.bfloat16)
        second = (project(wq2) * score_scale).astype(jnp.bfloat16)

        def put_q(head, value):
            q_out[head] = value

        joined(first, second, put_q)
        q_all[plane] = q_out[plane]
    z_start(("q", 1))
    loads[6].wait()
    begin(wo.at[core], wo.at[core], wo_send, wo_recv, me, 1 - core)
    loads[7].wait()
    loads[8].wait()

    tile = ROW_TILE
    tiles = rows // tile
    chunk = PLANE * rows
    lane = lax.broadcasted_iota(jnp.int32, (tile, width), 1)

    def pair_tile(group, key_group, part, diagonal):
        begin_row = pl.multiple_of(part * tile, tile)
        queries = q_all[group, pl.ds(begin_row, tile), :]
        zero = jnp.zeros_like(queries)
        both = jnp.concatenate(
            (jnp.where(lane < qk, queries, zero), jnp.where(lane >= qk, queries, zero)), axis=0
        )
        keys = k_all[pl.ds(key_group * PLANE, PLANE)].reshape(chunk, width)
        values = v_all[pl.ds(key_group * PLANE, PLANE)].reshape(chunk, head_v)
        scores = lax.dot_general(
            both, keys, (((1,), (1,)), ((), ())), preferred_element_type=jnp.float32
        )
        if diagonal:
            q_pos = (
                spot * rows
                + begin_row
                + lax.rem(lax.broadcasted_iota(jnp.int32, (2 * tile, chunk), 0), tile)
            )
            k_pos = lax.broadcasted_iota(jnp.int32, (2 * tile, chunk), 1)
            scores = jnp.where(k_pos <= q_pos, scores, masked_score)
        new_max = jnp.max(scores, axis=-1, keepdims=True)
        running_max = max_all[group, part]
        new_max = jnp.maximum(running_max, new_max)
        rescale = jnp.exp2(running_max - new_max)
        weights = jnp.exp2(scores - new_max)
        new_sum = jnp.sum(weights, axis=-1, keepdims=True)
        accum = jnp.dot(
            weights.astype(jnp.bfloat16), values, preferred_element_type=jnp.float32
        )
        max_all[group, part] = new_max
        sum_all[group, part] = sum_all[group, part] * rescale + new_sum
        acc_all[group, part] = acc_all[group, part] * rescale + accum

    def pair(group, key_group, diagonal):
        if not COMPUTE:
            return
        with scope("pair_d" if diagonal else "pair"):
            lax.fori_loop(
                0, tiles, lambda t, c: (pair_tile(group, key_group, t, diagonal), c)[1], 0
            )

    def meet(step, earlier):
        one, other = from_plane(step), from_plane(earlier)
        pair(jnp.maximum(one, other), jnp.minimum(one, other), False)

    def normed_copy(group):
        return send(
            n_out.at[group],
            n_all.at[core, plane],
            n_send.at[group],
            n_recv.at[plane],
            group * PLANE + spot,
            core,
        )

    def partner_copy(head):
        slot = n_all.at[core, head]
        return send(slot, slot, r_send.at[head], r_recv.at[head], me, 1 - core)

    lam = lam_ref[plane]
    gain = gain_ref[...]

    def finish(step):
        group = from_plane(step)
        if not COMPUTE:
            return

        def finish_tile(part, _):
            begin_row = pl.multiple_of(part * tile, tile)
            heads_out = acc_all[group, part] / sum_all[group, part]
            mixed = heads_out[:tile] - lam * heads_out[tile:]
            scale_rows = lax.rsqrt(jnp.mean(mixed * mixed, axis=-1, keepdims=True) + epsilon)
            normed = (mixed * scale_rows * gain).astype(jnp.bfloat16)
            n_out[group, pl.ds(begin_row, tile), :] = normed
            return 0

        lax.fori_loop(0, tiles, finish_tile, 0)

    def deliver(step):
        finish(step)
        group = from_plane(step)
        if step == 0:
            n_all[core, plane] = n_out[plane]
            partner_copy(plane).start()
        else:
            normed_copy(group).start()

    max_all[...] = jnp.full(max_all.shape, masked_score, jnp.float32)
    sum_all[...] = jnp.zeros(sum_all.shape, jnp.float32)
    acc_all[...] = jnp.zeros(acc_all.shape, jnp.float32)

    relay(0)
    gate(1)
    forward(1)
    ready(0)
    pair(plane, plane, True)
    forward(2)
    relay(1)
    gate(2)
    ready(1)
    ready_q(1)
    meet(1, 0)
    pair(from_plane(1), from_plane(1), True)
    relay(2)
    gate(3)
    forward(3)
    ready(2)
    ready_q(2)
    meet(2, 0)
    meet(2, 1)
    relay(3)
    pair(from_plane(2), from_plane(2), True)
    ready(3)
    ready_q(3)
    meet(3, 1)
    deliver(1)
    meet(3, 2)
    deliver(2)
    meet(3, 0)
    deliver(0)
    pair(from_plane(3), from_plane(3), True)
    deliver(3)

    for step in range(1, groups):
        head = from_plane(step)
        slot = n_all.at[core, head]
        with scope(f"n#s={step}"):
            arrived(slot, n_recv.at[head])
        partner_copy(head).start()

    def out_tiles(tp_index, first_part):
        normed = jnp.concatenate([n_all[tp_index, head] for head in range(groups)], axis=1)

        def out_tile(index, _):
            columns = pl.ds(pl.multiple_of(index * OUT_TILE, OUT_TILE), OUT_TILE)
            part = jnp.dot(normed, wo[tp_index, :, columns], preferred_element_type=jnp.float32)
            part = part.astype(jnp.bfloat16)
            if not first_part:
                part = (part.astype(jnp.float32) + out_ref[:, columns].astype(jnp.float32)).astype(
                    jnp.bfloat16
                )
            out_ref[:, columns] = part
            return 0

        lax.fori_loop(0, out_ref.shape[1] // OUT_TILE, out_tile, 0)

    with scope("out1"):
        out_tiles(core, True)
    with scope("rrecv"):
        arrived(wo.at[1 - core], wo_recv)
        for head in range(groups):
            arrived(n_all.at[1 - core, head], r_recv.at[head])
    with scope("out2"):
        out_tiles(1 - core, False)

    with scope("drain"):
        for copy in pending:
            copy.wait_send()
        pl.when(inner)(lambda: z_done(("v", 1)))
        for step in range(1, groups):
            z_done(("k", step), ("q", step))
            normed_copy(from_plane(step)).wait_send()
        for head in range(groups):
            partner_copy(head).wait_send()


COMPUTE = True


def fused_shards(
    hidden_in, query_one, query_two, key_one, key_two, value_proj, lambdas, norm_gain, out_proj
):
    groups = lambdas.shape[0]
    rows, depth = hidden_in.shape
    head_qk = query_one.shape[1] // groups
    head_v = value_proj.shape[1] // groups
    width = 2 * head_qk
    blocks = groups * PLANE
    columns = out_proj.shape[1]
    score_scale = 1.75 * head_qk ** (-0.5) * math.log2(math.e)
    bf16 = jnp.bfloat16
    dma = pltpu.SemaphoreType.DMA
    hbm = pl.BlockSpec(memory_space=pltpu.HBM)
    vmem = pl.BlockSpec(memory_space=pltpu.VMEM)

    def body(*refs):
        fused_kernel(groups, score_scale, *refs)

    return pl.pallas_call(
        body,
        name="fused_attention",
        out_shape=jax.ShapeDtypeStruct((rows, columns), bf16),
        in_specs=[hbm] * 9,
        out_specs=vmem,
        scratch_shapes=[
            pltpu.VMEM(hidden_in.shape, bf16),
            pltpu.VMEM(query_one.shape, bf16),
            pltpu.VMEM(query_two.shape, bf16),
            pltpu.VMEM(key_one.shape, bf16),
            pltpu.VMEM(key_two.shape, bf16),
            pltpu.VMEM(value_proj.shape, bf16),
            pltpu.VMEM((2,) + out_proj.shape, bf16),
            pltpu.SMEM(lambdas.shape, jnp.float32),
            pltpu.VMEM((1, head_v), jnp.float32),
            pltpu.VMEM((groups, rows, width), bf16),
            pltpu.VMEM((groups, rows, head_v), bf16),
            pltpu.VMEM((groups, rows, width), bf16),
            pltpu.VMEM((blocks, rows, width), bf16),
            pltpu.VMEM((blocks, rows, head_v), bf16),
            pltpu.VMEM((groups, rows, width), bf16),
            pltpu.VMEM((groups, rows, head_v), bf16),
            pltpu.VMEM((2, groups, rows, head_v), bf16),
            pltpu.VMEM((groups, rows // ROW_TILE, 2 * ROW_TILE, 1), jnp.float32),
            pltpu.VMEM((groups, rows // ROW_TILE, 2 * ROW_TILE, 1), jnp.float32),
            pltpu.VMEM((groups, rows // ROW_TILE, 2 * ROW_TILE, head_v), jnp.float32),
            dma((9,)),
            dma,
            dma,
        ]
        + [dma((groups,))] * 22,
        compiler_params=pltpu.CompilerParams(
            collective_id=0, has_side_effects=True, vmem_limit_bytes=VMEM_LIMIT
        ),
    )(
        *(
            pltpu.with_memory_space_constraint(item, pltpu.HBM)
            for item in (
                hidden_in,
                query_one,
                query_two,
                key_one,
                key_two,
                value_proj,
                lambdas,
                norm_gain.reshape(1, head_v),
                out_proj,
            )
        )
    )


VMEM_LIMIT = 48 * 1024 * 1024


def solution(mesh):
    placed = (
        P("sp", None),
        P(None, "tp"),
        P(None, "tp"),
        P(None, "tp"),
        P(None, "tp"),
        P(None, "tp"),
        P("tp"),
        P(),
        P("tp", None),
    )

    def body(*args):
        groups = args[6].shape[0]
        split = groups * PLANE == mesh.shape["sp"] and mesh.shape["tp"] == 2
        return (fused_shards if split else shards)(*args)

    return jax.shard_map(
        body, mesh=mesh, in_specs=placed, out_specs=P("sp", None), check_vma=False
    )
```

time: 55.7 us -> 49 us (0.88)
  Pallas kernels: 53.2 us -> 47.8 us
  local copies, waits for them, and re-layouts: 2.3 us -> 0.97 us
    pallas_call x1, Pallas kernels: 53.2 us -> 47.8 us  [fused_shards(): pl.pallas_call(body, name='fused_attention', out_shape=jax.ShapeDtypeStru...]
    unnamed x1, local copies, waits for them, and re-layouts: 2.3 us -> 0.97 us
where the time goes in v1:
time: 49 us; the launch traced here: 48.8 us
  Pallas kernels  47.8 us (98%)
  local copies, waits for them, and re-layouts  0.97 us (2%)
    pallas_call x1, Pallas kernels, fused_shards(): pl.pallas_call(body, name='fused_attention', out_shape=jax.ShapeDtypeStru...  47.8 us

profile of v1, /device:TPU:0, one launch (start us, length us, event | category | flops | bytes accessed | tf_op | source)
XLA Modules:
  0.0 48.8 jit_solution(14394906674127823059)
XLA Ops:
  0.0 47.8 %fused_attention.1 = bf16[256,2048]{1,0:T(8,128)(2,1)S(1)} custom-call(bf16[256,2048]{1,0:T(8,128)(2,1)} %refs_0_.1, bf16[2048,256]{1,0:T(8,128)(2,1)} %refs_1_.1, bf16[2048,256]{1,0:T(8,128)(2,1)} %refs_2_.1, bf16[2048,256]{1,0:T(8,128)(2,1)} %refs_3_.1, bf16[2048,256]{1,0:T(8,128)(2,1)} %refs_4_.1, bf16[2048,512]{1,0:T(8,128)(2,1)} %refs_5_.1, f32[4]{0:T(128)} %refs_6_.1, ...), custom_call_target="tpu_custom_call" | custom-call | tf_op jit(solution)/shard_map/fused_attention/pallas_call | solution.py:594
  47.8 1.0 %copy.11 = bf16[256,2048]{1,0:T(8,128)(2,1)} copy(bf16[256,2048]{1,0:T(8,128)(2,1)S(1)} %fused_attention.1) | data formatting | bytes 2097152

commit v2 on v1

--- a/solution.py
+++ b/solution.py
@@ -115,6 +115,7 @@
 PLANE = 4
 ROW_TILE = 256
 OUT_TILE = 1024
+LANES = 128
 
 
 def fused_kernel(
@@ -293,15 +294,11 @@
                 else:
                     z_start(*(("q", step) for step in far))
 
-            if index < groups - 1:
+            if index == groups - 1:
 
                 @pl.when(inner)
                 def _():
-                    z_done(("v", index + 1))
-                    if index + 1 < groups - 1:
-                        z_start(("k", index + 2), ("v", index + 2))
-                    else:
-                        z_start(*(("q", step) for step in far))
+                    z_start(*(("q", step) for step in far))
 
     def x_block(step):
         return from_plane(step) * PLANE + x_spot
@@ -368,7 +365,7 @@
     with scope("barrier"):
         pl.semaphore_wait(barrier, groups - 1 + 3)
     z_start(("k", 1))
-    pl.when(inner)(lambda: z_start(("k", 2)))
+    pl.when(inner)(lambda: z_start(*(("k", step) for step in far)))
     spread_k(0)
     with scope("w_v"):
         loads[3].wait()
@@ -378,7 +375,7 @@
             v_out[head] = value[:, head * head_v : (head + 1) * head_v]
         v_all[me] = v_out[plane]
     z_start(("v", 1))
-    pl.when(inner)(lambda: z_start(("v", 2)))
+    pl.when(inner)(lambda: z_start(*(("v", step) for step in far)))
     spread_v(0)
     with scope("w_q"):
         loads[4].wait()
@@ -415,22 +412,33 @@
         scores = lax.dot_general(
             both, keys, (((1,), (1,)), ((), ())), preferred_element_type=jnp.float32
         )
+        cuts = [scores[:, c * LANES : (c + 1) * LANES] for c in range(chunk // LANES)]
         if diagonal:
-            q_pos = (
+            row = lax.rem(lax.broadcasted_iota(jnp.int32, (2 * tile, LANES), 0), tile)
+            slack = (
                 spot * rows
                 + begin_row
-                + lax.rem(lax.broadcasted_iota(jnp.int32, (2 * tile, chunk), 0), tile)
+                + row
+                - lax.broadcasted_iota(jnp.int32, (2 * tile, LANES), 1)
             )
-            k_pos = lax.broadcasted_iota(jnp.int32, (2 * tile, chunk), 1)
-            scores = jnp.where(k_pos <= q_pos, scores, masked_score)
-        new_max = jnp.max(scores, axis=-1, keepdims=True)
+            cuts = [jnp.where(slack >= c * LANES, cut, masked_score) for c, cut in enumerate(cuts)]
+        highest = cuts[0]
+        for cut in cuts[1:]:
+            highest = jnp.maximum(highest, cut)
         running_max = max_all[group, part]
-        new_max = jnp.maximum(running_max, new_max)
+        new_max = jnp.maximum(
+            running_max,
+            jnp.broadcast_to(jnp.max(highest, axis=-1, keepdims=True), highest.shape),
+        )
         rescale = jnp.exp2(running_max - new_max)
-        weights = jnp.exp2(scores - new_max)
-        new_sum = jnp.sum(weights, axis=-1, keepdims=True)
+        weights = [jnp.exp2(cut - new_max) for cut in cuts]
+        new_sum = weights[0]
+        for weight in weights[1:]:
+            new_sum = new_sum + weight
         accum = jnp.dot(
-            weights.astype(jnp.bfloat16), values, preferred_element_type=jnp.float32
+            jnp.concatenate([weight.astype(jnp.bfloat16) for weight in weights], axis=1),
+            values,
+            preferred_element_type=jnp.float32,
         )
         max_all[group, part] = new_max
         sum_all[group, part] = sum_all[group, part] * rescale + new_sum
@@ -472,7 +480,9 @@
 
         def finish_tile(part, _):
             begin_row = pl.multiple_of(part * tile, tile)
-            heads_out = acc_all[group, part] / sum_all[group, part]
+            heads_out = acc_all[group, part] / jnp.sum(
+                sum_all[group, part], axis=-1, keepdims=True
+            )
             mixed = heads_out[:tile] - lam * heads_out[tile:]
             scale_rows = lax.rsqrt(jnp.mean(mixed * mixed, axis=-1, keepdims=True) + epsilon)
             normed = (mixed * scale_rows * gain).astype(jnp.bfloat16)
@@ -561,7 +571,7 @@
     with scope("drain"):
         for copy in pending:
             copy.wait_send()
-        pl.when(inner)(lambda: z_done(("v", 1)))
+        pl.when(inner)(lambda: z_done(*(("v", step) for step in range(1, groups))))
         for step in range(1, groups):
             z_done(("k", step), ("q", step))
             normed_copy(from_plane(step)).wait_send()
@@ -615,8 +625,8 @@
             pltpu.VMEM((groups, rows, width), bf16),
             pltpu.VMEM((groups, rows, head_v), bf16),
             pltpu.VMEM((2, groups, rows, head_v), bf16),
-            pltpu.VMEM((groups, rows // ROW_TILE, 2 * ROW_TILE, 1), jnp.float32),
-            pltpu.VMEM((groups, rows // ROW_TILE, 2 * ROW_TILE, 1), jnp.float32),
+            pltpu.VMEM((groups, rows // ROW_TILE, 2 * ROW_TILE, LANES), jnp.float32),
+            pltpu.VMEM((groups, rows // ROW_TILE, 2 * ROW_TILE, LANES), jnp.float32),
             pltpu.VMEM((groups, rows // ROW_TILE, 2 * ROW_TILE, head_v), jnp.float32),
             dma((9,)),
             dma,

time: 49 us -> 44.8 us (0.914)
  Pallas kernels: 47.8 us -> 43.7 us
    pallas_call x1, Pallas kernels: 47.8 us -> 43.7 us  [fused_shards(): pl.pallas_call(body, name='fused_attention', out_shape=jax.ShapeDtypeStru...]
where the time goes in v2:
time: 44.8 us; the launch traced here: 44.7 us
  Pallas kernels  43.7 us (98%)
  local copies, waits for them, and re-layouts  0.97 us (2%)
    pallas_call x1, Pallas kernels, fused_shards(): pl.pallas_call(body, name='fused_attention', out_shape=jax.ShapeDtypeStru...  43.7 us
    unnamed x1, local copies, waits for them, and re-layouts  0.97 us

profile of v2, /device:TPU:0, one launch (start us, length us, event | category | flops | bytes accessed | tf_op | source)
XLA Modules:
  0.0 44.7 jit_solution(5840360812013057258)
XLA Ops:
  0.0 43.7 %fused_attention.1 = bf16[256,2048]{1,0:T(8,128)(2,1)S(1)} custom-call(bf16[256,2048]{1,0:T(8,128)(2,1)} %refs_0_.1, bf16[2048,256]{1,0:T(8,128)(2,1)} %refs_1_.1, bf16[2048,256]{1,0:T(8,128)(2,1)} %refs_2_.1, bf16[2048,256]{1,0:T(8,128)(2,1)} %refs_3_.1, bf16[2048,256]{1,0:T(8,128)(2,1)} %refs_4_.1, bf16[2048,512]{1,0:T(8,128)(2,1)} %refs_5_.1, f32[4]{0:T(128)} %refs_6_.1, ...), custom_call_target="tpu_custom_call" | custom-call | tf_op jit(solution)/shard_map/fused_attention/pallas_call | solution.py:604
  43.7 1.0 %copy.11 = bf16[256,2048]{1,0:T(8,128)(2,1)} copy(bf16[256,2048]{1,0:T(8,128)(2,1)S(1)} %fused_attention.1) | data formatting | bytes 2097152

commit v3 on v2

--- a/solution.py
+++ b/solution.py
@@ -237,14 +237,14 @@
     def arrived(ref, recv_sem):
         pltpu.make_async_copy(ref, ref, recv_sem).wait()
 
-    upper = plane >= groups // 2
-    mirrored = jnp.where(upper, groups - 1 - plane, plane)
-
+    half = groups // 2
+    upper = plane >= half
+    lower = jnp.logical_not(upper)
+    base = jnp.where(upper, half, 0)
     def from_plane(step):
-        if step == 0:
-            return plane
-        near = jnp.where(step - 1 < mirrored, step - 1, step)
-        return jnp.where(upper, groups - 1 - near, near)
+        if step < half:
+            return base + lax.rem(plane + step, half)
+        return (half - base) + (step - half)
 
     def project(weight_ref):
         return jnp.dot(hid[...], weight_ref[...], preferred_element_type=jnp.float32)
@@ -253,9 +253,6 @@
         for head in range(groups):
             cut = slice(head * qk, (head + 1) * qk)
             store(head, jnp.concatenate((first[:, cut], second[:, cut]), axis=1))
-
-    outer = jnp.logical_or(plane == 0, plane == groups - 1)
-    inner = jnp.logical_not(outer)
 
     def z_copy(kind, step):
         target = from_plane(step)
@@ -281,24 +278,14 @@
         for kind, step in items:
             z_copy(kind, step).wait_send()
 
-    far = [step for step in range(2, groups)]
-
-    def gate(index):
-        with scope(f"gate#{index}"):
-
-            @pl.when(outer)
-            def _():
-                z_done(("v", index))
-                if index < groups - 1:
-                    z_start(("k", index + 1), ("v", index + 1))
-                else:
-                    z_start(*(("q", step) for step in far))
-
-            if index == groups - 1:
-
-                @pl.when(inner)
+    def launch(moment):
+        for index in range(groups):
+            items = SENDS[index].get(moment, "").split()
+            if items:
+
+                @pl.when(plane == index)
                 def _():
-                    z_start(*(("q", step) for step in far))
+                    z_start(*((item[0], int(item[1])) for item in items))
 
     def x_block(step):
         return from_plane(step) * PLANE + x_spot
@@ -364,8 +351,7 @@
         k_all[me] = k_out[plane]
     with scope("barrier"):
         pl.semaphore_wait(barrier, groups - 1 + 3)
-    z_start(("k", 1))
-    pl.when(inner)(lambda: z_start(*(("k", step) for step in far)))
+    launch("k")
     spread_k(0)
     with scope("w_v"):
         loads[3].wait()
@@ -374,8 +360,7 @@
         for head in range(groups):
             v_out[head] = value[:, head * head_v : (head + 1) * head_v]
         v_all[me] = v_out[plane]
-    z_start(("v", 1))
-    pl.when(inner)(lambda: z_start(*(("v", step) for step in far)))
+    launch("v")
     spread_v(0)
     with scope("w_q"):
         loads[4].wait()
@@ -389,7 +374,7 @@
 
         joined(first, second, put_q)
         q_all[plane] = q_out[plane]
-    z_start(("q", 1))
+    launch("q")
     loads[6].wait()
     begin(wo.at[core], wo.at[core], wo_send, wo_recv, me, 1 - core)
     loads[7].wait()
@@ -504,37 +489,57 @@
     sum_all[...] = jnp.zeros(sum_all.shape, jnp.float32)
     acc_all[...] = jnp.zeros(acc_all.shape, jnp.float32)
 
+    def diagonal(step):
+        pair(from_plane(step), from_plane(step), True)
+
     relay(0)
-    gate(1)
     forward(1)
+    launch("c")
     ready(0)
-    pair(plane, plane, True)
+    launch("d")
+    diagonal(0)
     forward(2)
     relay(1)
-    gate(2)
+    launch("e")
     ready(1)
+    launch("f")
     ready_q(1)
     meet(1, 0)
-    pair(from_plane(1), from_plane(1), True)
+    diagonal(1)
+
     relay(2)
-    gate(3)
     forward(3)
+
+    @pl.when(lower)
+    def _():
+        deliver(1)
+        deliver(0)
+
     ready(2)
     ready_q(2)
     meet(2, 0)
     meet(2, 1)
+    diagonal(2)
+    deliver(2)
     relay(3)
-    pair(from_plane(2), from_plane(2), True)
+    ready_q(3)
+    meet(3, 2)
+
+    @pl.when(lower)
+    def _():
+        meet(3, 0)
+        meet(3, 1)
+
     ready(3)
-    ready_q(3)
-    meet(3, 1)
-    deliver(1)
-    meet(3, 2)
-    deliver(2)
-    meet(3, 0)
-    deliver(0)
-    pair(from_plane(3), from_plane(3), True)
+    diagonal(3)
     deliver(3)
+
+    @pl.when(upper)
+    def _():
+        meet(3, 1)
+        deliver(1)
+        meet(3, 0)
+        deliver(0)
 
     for step in range(1, groups):
         head = from_plane(step)
@@ -571,15 +576,20 @@
     with scope("drain"):
         for copy in pending:
             copy.wait_send()
-        pl.when(inner)(lambda: z_done(*(("v", step) for step in range(1, groups))))
         for step in range(1, groups):
-            z_done(("k", step), ("q", step))
+            z_done(("k", step), ("v", step), ("q", step))
             normed_copy(from_plane(step)).wait_send()
         for head in range(groups):
             partner_copy(head).wait_send()
 
 
 COMPUTE = True
+SENDS = (
+    {"k": "k1", "v": "v1 k3 v3 k2 v2", "q": "q1", "f": "q2 q3"},
+    {"k": "k1 k2", "v": "v1 v2 k3 v3", "q": "q1 q2 q3"},
+    {"k": "k1 k3", "v": "v1 v3 k2 v2", "q": "q1 q3 q2"},
+    {"k": "k1", "v": "v1", "q": "q1", "d": "k3 v3 k2 v2 q3 q2"},
+)
 
 
 def fused_shards(

time: 44.8 us -> 39.7 us (0.89)
  the two profiles are of different devices: /device:TPU:0 before, /device:TPU:17 now
where the time goes in v3:
time: 39.7 us; the launch traced here: 39.6 us
  Pallas kernels  38.6 us (97%)
  local copies, waits for them, and re-layouts  0.97 us (2%)
    pallas_call x1, Pallas kernels, fused_shards(): pl.pallas_call(body, name='fused_attention', out_shape=jax.ShapeDtypeStru...  38.6 us
    unnamed x1, local copies, waits for them, and re-layouts  0.97 us

profile of v3, /device:TPU:17, one launch (start us, length us, event | category | flops | bytes accessed | tf_op | source)
XLA Modules:
  0.0 39.6 jit_solution(10473671469142756447)
XLA Ops:
  0.0 38.6 %fused_attention.1 = bf16[256,2048]{1,0:T(8,128)(2,1)S(1)} custom-call(bf16[256,2048]{1,0:T(8,128)(2,1)} %refs_0_.1, bf16[2048,256]{1,0:T(8,128)(2,1)} %refs_1_.1, bf16[2048,256]{1,0:T(8,128)(2,1)} %refs_2_.1, bf16[2048,256]{1,0:T(8,128)(2,1)} %refs_3_.1, bf16[2048,256]{1,0:T(8,128)(2,1)} %refs_4_.1, bf16[2048,512]{1,0:T(8,128)(2,1)} %refs_5_.1, f32[4]{0:T(128)} %refs_6_.1, ...), custom_call_target="tpu_custom_call" | custom-call | tf_op jit(solution)/shard_map/fused_attention/pallas_call | solution.py:614
  38.6 1.0 %copy.11 = bf16[256,2048]{1,0:T(8,128)(2,1)} copy(bf16[256,2048]{1,0:T(8,128)(2,1)S(1)} %fused_attention.1) | data formatting | bytes 2097152

commit v4 on v3

--- a/solution.py
+++ b/solution.py
@@ -1,3 +1,4 @@
+import functools
 import math
 
 import jax
@@ -114,7 +115,7 @@
 MESH = pl.DeviceIdType.MESH
 PLANE = 4
 ROW_TILE = 256
-OUT_TILE = 1024
+OUT_TILE = 2048
 LANES = 128
 
 
@@ -139,6 +140,7 @@
     wv,
     wo,
     lam_ref,
+    lam_all,
     gain_ref,
     k_out,
     v_out,
@@ -151,9 +153,12 @@
     max_all,
     sum_all,
     acc_all,
+    out_acc,
     load_sem,
     wo_send,
     wo_recv,
+    lam_send,
+    lam_recv,
     zk_send,
     zk_recv,
     zv_send,
@@ -182,8 +187,11 @@
     core = lax.axis_index("tp")
     plane = me // PLANE
     spot = lax.rem(me, PLANE)
-    x_spot = spot + 1 - 2 * lax.rem(spot, 2)
-    y_spot = spot + 2 - 4 * (spot // 2)
+    x = lax.rem(spot, 2)
+    y = spot // 2
+    mine = 2 * core + x
+    home = core == y
+    away = core != y
     rows = hid.shape[0]
     qk = q1_hbm.shape[1] // groups
     width = 2 * qk
@@ -210,14 +218,14 @@
     def greet(index, tp_index):
         pl.semaphore_signal(barrier, inc=1, device_id=(index, tp_index), device_id_type=MESH)
 
+    def owner(index):
+        return index * PLANE + mine, y
+
     for step in range(1, groups):
-        other = lax.rem(plane + step, groups) * PLANE + spot
-        greet(other, core)
+        greet(*owner(lax.rem(plane + step, groups)))
+    pl.when(away)(lambda: greet(*owner(plane)))
     greet(me, 1 - core)
-    greet(plane * PLANE + x_spot, core)
-    greet(plane * PLANE + y_spot, core)
-
-    pending = []
+    greet(me + 1 - 2 * x, core)
 
     def send(src, dst, send_sem, recv_sem, index, tp_index):
         return pltpu.make_async_remote_copy(
@@ -229,11 +237,6 @@
             device_id_type=MESH,
         )
 
-    def begin(*args):
-        copy = send(*args)
-        copy.start()
-        pending.append(copy)
-
     def arrived(ref, recv_sem):
         pltpu.make_async_copy(ref, ref, recv_sem).wait()
 
@@ -241,10 +244,12 @@
     upper = plane >= half
     lower = jnp.logical_not(upper)
     base = jnp.where(upper, half, 0)
+    swapped = lax.rem(plane, half) == 0
+
     def from_plane(step):
         if step < half:
             return base + lax.rem(plane + step, half)
-        return (half - base) + (step - half)
+        return (half - base) + jnp.where(swapped, groups - 1 - step, step - half)
 
     def project(weight_ref):
         return jnp.dot(hid[...], weight_ref[...], preferred_element_type=jnp.float32)
@@ -266,8 +271,7 @@
             full,
             sems.at[step],
             recvs.at[plane],
-            target * PLANE + spot,
-            core,
+            *owner(target),
         )
 
     def z_start(*items):
@@ -278,55 +282,83 @@
         for kind, step in items:
             z_copy(kind, step).wait_send()
 
-    def launch(moment):
-        for index in range(groups):
-            items = SENDS[index].get(moment, "").split()
+    def perform(items):
+        for item in items:
+            kind, step = item[0], int(item[1])
+            if kind in "kvq":
+                z_copy(kind, step).start()
+            else:
+                {"z": forward, "r": relay, "w": ready, "a": ready_q}[kind](step)
+
+    places = [
+        jnp.logical_and(plane == index, place) for index in range(groups) for place in (home, away)
+    ]
+
+    def moment(name):
+        texts = [order.get(name, "") for order in ORDER]
+        lists = [[text[i : i + 2] for i in range(0, len(text), 2)] for text in texts]
+        if all(items == lists[0] for items in lists):
+            perform(lists[0])
+            return
+        for items in dict.fromkeys(map(tuple, lists)):
             if items:
-
-                @pl.when(plane == index)
-                def _():
-                    z_start(*((item[0], int(item[1])) for item in items))
+                place = functools.reduce(
+                    jnp.logical_or, [p for p, other in zip(places, lists) if tuple(other) == items]
+                )
+                pl.when(place)(lambda items=items: perform(items))
 
     def x_block(step):
-        return from_plane(step) * PLANE + x_spot
+        return from_plane(step) * PLANE + mine + 1 - 2 * x
 
     def y_block(step):
-        return from_plane(step) * PLANE + y_spot
+        return from_plane(step) * PLANE + mine + 2 - 4 * core
+
+    def to_x(slot, sems, recvs, step):
+        return send(slot, slot, sems.at[step], recvs.at[step], me + 1 - 2 * x, core)
+
+    def to_y(slot, sems, recvs, step):
+        return send(slot, slot, sems.at[step], recvs.at[step], me, 1 - core)
 
     def spread_k(step):
-        slot = k_all.at[from_plane(step) * PLANE + spot]
-        begin(slot, slot, xk_send.at[step], xk_recv.at[step], plane * PLANE + x_spot, core)
-        begin(slot, slot, yk_send.at[step], yk_recv.at[step], plane * PLANE + y_spot, core)
+        slot = k_all.at[from_plane(step) * PLANE + mine]
+        return (to_x(slot, xk_send, xk_recv, step), to_y(slot, yk_send, yk_recv, step))
 
     def spread_v(step):
-        slot = v_all.at[from_plane(step) * PLANE + spot]
-        begin(slot, slot, yv_send.at[step], yv_recv.at[step], plane * PLANE + y_spot, core)
-        begin(slot, slot, xv_send.at[step], xv_recv.at[step], plane * PLANE + x_spot, core)
+        slot = v_all.at[from_plane(step) * PLANE + mine]
+        return (to_x(slot, xv_send, xv_recv, step), to_y(slot, yv_send, yv_recv, step))
+
+    def relay_k(step):
+        return (to_y(k_all.at[x_block(step)], fk_send, fk_recv, step),)
+
+    def relay_v(step):
+        return (to_y(v_all.at[x_block(step)], fv_send, fv_recv, step),)
+
+    def start(copies):
+        for copy in copies:
+            copy.start()
 
     def forward(step):
         source = from_plane(step)
         with scope(f"zk#s={step}"):
-            arrived(k_all.at[source * PLANE + spot], zk_recv.at[source])
-        spread_k(step)
+            arrived(k_all.at[source * PLANE + mine], zk_recv.at[source])
+        start(spread_k(step))
         with scope(f"zv#s={step}"):
-            arrived(v_all.at[source * PLANE + spot], zv_recv.at[source])
-        spread_v(step)
+            arrived(v_all.at[source * PLANE + mine], zv_recv.at[source])
+        start(spread_v(step))
 
     def relay(step):
         with scope(f"rk#s={step}"):
-            slot = k_all.at[x_block(step)]
-            arrived(slot, xk_recv.at[step])
-        begin(slot, slot, fk_send.at[step], fk_recv.at[step], plane * PLANE + y_spot, core)
+            arrived(k_all.at[x_block(step)], xk_recv.at[step])
+        start(relay_k(step))
         with scope(f"rv#s={step}"):
-            slot = v_all.at[y_block(step)]
-            arrived(slot, yv_recv.at[step])
-        begin(slot, slot, fv_send.at[step], fv_recv.at[step], plane * PLANE + x_spot, core)
+            arrived(v_all.at[x_block(step)], xv_recv.at[step])
+        start(relay_v(step))
 
     def ready(step):
-        far = from_plane(step) * PLANE + (PLANE - 1 - spot)
+        far = from_plane(step) * PLANE + (PLANE - 1 - mine)
         with scope(f"ready#s={step}"):
-            arrived(v_all.at[x_block(step)], xv_recv.at[step])
             arrived(k_all.at[y_block(step)], yk_recv.at[step])
+            arrived(v_all.at[y_block(step)], yv_recv.at[step])
             arrived(k_all.at[far], fk_recv.at[step])
             arrived(v_all.at[far], fv_recv.at[step])
 
@@ -348,20 +380,28 @@
             k_out[head] = value
 
         joined(first, second, put_k)
-        k_all[me] = k_out[plane]
+
+        @pl.when(home)
+        def _():
+            k_all[me] = k_out[plane]
+
     with scope("barrier"):
-        pl.semaphore_wait(barrier, groups - 1 + 3)
-    launch("k")
-    spread_k(0)
+        pl.semaphore_wait(barrier, groups - 1 + 2 + jnp.where(away, 1, 0))
+    pl.when(home)(lambda: start(spread_k(0)))
+    moment("k")
     with scope("w_v"):
         loads[3].wait()
     with scope("p_v"):
         value = project(wv).astype(jnp.bfloat16)
         for head in range(groups):
             v_out[head] = value[:, head * head_v : (head + 1) * head_v]
-        v_all[me] = v_out[plane]
-    launch("v")
-    spread_v(0)
+
+        @pl.when(home)
+        def _():
+            v_all[me] = v_out[plane]
+
+    pl.when(home)(lambda: start(spread_v(0)))
+    moment("v")
     with scope("w_q"):
         loads[4].wait()
         loads[5].wait()
@@ -373,12 +413,21 @@
             q_out[head] = value
 
         joined(first, second, put_q)
-        q_all[plane] = q_out[plane]
-    launch("q")
+
+        @pl.when(home)
+        def _():
+            q_all[plane] = q_out[plane]
+
+    moment("q")
     loads[6].wait()
-    begin(wo.at[core], wo.at[core], wo_send, wo_recv, me, 1 - core)
+    wo_copy = send(wo.at[core], wo.at[core], wo_send, wo_recv, me, 1 - core)
+    wo_copy.start()
     loads[7].wait()
     loads[8].wait()
+    for head in range(groups):
+        lam_all[core, head] = jnp.full(lam_all.shape[2:], lam_ref[head], jnp.float32)
+    lam_copy = send(lam_all.at[core], lam_all.at[core], lam_send, lam_recv, me, 1 - core)
+    lam_copy.start()
 
     tile = ROW_TILE
     tiles = rows // tile
@@ -401,7 +450,7 @@
         if diagonal:
             row = lax.rem(lax.broadcasted_iota(jnp.int32, (2 * tile, LANES), 0), tile)
             slack = (
-                spot * rows
+                mine * rows
                 + begin_row
                 + row
                 - lax.broadcasted_iota(jnp.int32, (2 * tile, LANES), 1)
@@ -444,18 +493,16 @@
     def normed_copy(group):
         return send(
             n_out.at[group],
-            n_all.at[core, plane],
+            n_all.at[y, plane],
             n_send.at[group],
             n_recv.at[plane],
-            group * PLANE + spot,
-            core,
+            *owner(group),
         )
 
     def partner_copy(head):
         slot = n_all.at[core, head]
         return send(slot, slot, r_send.at[head], r_recv.at[head], me, 1 - core)
 
-    lam = lam_ref[plane]
     gain = gain_ref[...]
 
     def finish(step):
@@ -468,7 +515,7 @@
             heads_out = acc_all[group, part] / jnp.sum(
                 sum_all[group, part], axis=-1, keepdims=True
             )
-            mixed = heads_out[:tile] - lam * heads_out[tile:]
+            mixed = heads_out[:tile] - lam_all[y, plane][:1] * heads_out[tile:]
             scale_rows = lax.rsqrt(jnp.mean(mixed * mixed, axis=-1, keepdims=True) + epsilon)
             normed = (mixed * scale_rows * gain).astype(jnp.bfloat16)
             n_out[group, pl.ds(begin_row, tile), :] = normed
@@ -480,8 +527,16 @@
         finish(step)
         group = from_plane(step)
         if step == 0:
-            n_all[core, plane] = n_out[plane]
-            partner_copy(plane).start()
+
+            @pl.when(home)
+            def _():
+                n_all[core, plane] = n_out[plane]
+                partner_copy(plane).start()
+
+            @pl.when(away)
+            def _():
+                normed_copy(group).start()
+
         else:
             normed_copy(group).start()
 
@@ -492,47 +547,56 @@
     def diagonal(step):
         pair(from_plane(step), from_plane(step), True)
 
-    relay(0)
-    forward(1)
-    launch("c")
-    ready(0)
-    launch("d")
+    moment("0")
+    arrived(lam_all.at[1 - core], lam_recv)
     diagonal(0)
-    forward(2)
-    relay(1)
-    launch("e")
-    ready(1)
-    launch("f")
-    ready_q(1)
+    moment("1")
     meet(1, 0)
     diagonal(1)
-
-    relay(2)
-    forward(3)
 
     @pl.when(lower)
     def _():
         deliver(1)
         deliver(0)
 
-    ready(2)
-    ready_q(2)
+    moment("2")
     meet(2, 0)
+    moment("2a")
     meet(2, 1)
+    moment("2b")
     diagonal(2)
-    deliver(2)
-    relay(3)
-    ready_q(3)
-    meet(3, 2)
+
+    @pl.when(jnp.logical_not(swapped))
+    def _():
+        deliver(2)
+
+    moment("3")
+
+    @pl.when(jnp.logical_not(swapped))
+    def _():
+        meet(3, 2)
+
+    moment("3a")
 
     @pl.when(lower)
     def _():
         meet(3, 0)
         meet(3, 1)
 
-    ready(3)
+    moment("4")
+
+    @pl.when(jnp.logical_and(swapped, lower))
+    def _():
+        meet(3, 2)
+        deliver(2)
+
     diagonal(3)
     deliver(3)
+
+    @pl.when(jnp.logical_and(swapped, upper))
+    def _():
+        meet(3, 2)
+        deliver(2)
 
     @pl.when(upper)
     def _():
@@ -541,41 +605,60 @@
         meet(3, 0)
         deliver(0)
 
-    for step in range(1, groups):
-        head = from_plane(step)
-        slot = n_all.at[core, head]
-        with scope(f"n#s={step}"):
-            arrived(slot, n_recv.at[head])
-        partner_copy(head).start()
-
-    def out_tiles(tp_index, first_part):
-        normed = jnp.concatenate([n_all[tp_index, head] for head in range(groups)], axis=1)
-
-        def out_tile(index, _):
-            columns = pl.ds(pl.multiple_of(index * OUT_TILE, OUT_TILE), OUT_TILE)
-            part = jnp.dot(normed, wo[tp_index, :, columns], preferred_element_type=jnp.float32)
-            part = part.astype(jnp.bfloat16)
-            if not first_part:
-                part = (part.astype(jnp.float32) + out_ref[:, columns].astype(jnp.float32)).astype(
-                    jnp.bfloat16
+    def collect(head):
+        @pl.when(jnp.logical_or(plane != head, away))
+        def _():
+            slot = n_all.at[core, head]
+            with scope(f"n#h={head}"):
+                arrived(slot, n_recv.at[head])
+            partner_copy(head).start()
+
+    def out_part(tp_index, first, last):
+        heads = slice(first * head_v, (first + half) * head_v)
+        with scope(f"out#f={first}"):
+            normed = jnp.concatenate(
+                [n_all[tp_index, head] for head in range(first, first + half)], axis=1
+            )
+
+            def out_tile(index, _):
+                columns = pl.ds(pl.multiple_of(index * OUT_TILE, OUT_TILE), OUT_TILE)
+                part = jnp.dot(
+                    normed, wo[tp_index, heads, columns], preferred_element_type=jnp.float32
                 )
-            out_ref[:, columns] = part
-            return 0
-
-        lax.fori_loop(0, out_ref.shape[1] // OUT_TILE, out_tile, 0)
-
-    with scope("out1"):
-        out_tiles(core, True)
-    with scope("rrecv"):
-        arrived(wo.at[1 - core], wo_recv)
-        for head in range(groups):
-            arrived(n_all.at[1 - core, head], r_recv.at[head])
-    with scope("out2"):
-        out_tiles(1 - core, False)
+                if last is not None:
+                    part = part + out_acc[:, columns]
+                if last:
+                    out_ref[:, columns] = part.astype(jnp.bfloat16)
+                else:
+                    out_acc[:, columns] = part
+                return 0
+
+            lax.fori_loop(0, out_ref.shape[1] // OUT_TILE, out_tile, 0)
+
+    for first in range(0, groups, half):
+        for head in range(first, first + half):
+            collect(head)
+        out_part(core, first, None if first == 0 else False)
+    arrived(wo.at[1 - core], wo_recv)
+    for first in range(0, groups, half):
+        with scope(f"rrecv#f={first}"):
+            for head in range(first, first + half):
+                arrived(n_all.at[1 - core, head], r_recv.at[head])
+        out_part(1 - core, first, first + half == groups)
 
     with scope("drain"):
-        for copy in pending:
-            copy.wait_send()
+        wo_copy.wait_send()
+        lam_copy.wait_send()
+        for step in range(groups):
+            for copies in (spread_k, spread_v, relay_k, relay_v):
+                for copy in copies(step):
+                    copy.wait_send()
+
+        @pl.when(away)
+        def _():
+            z_done(("k", 0), ("v", 0), ("q", 0))
+            normed_copy(plane).wait_send()
+
         for step in range(1, groups):
             z_done(("k", step), ("v", step), ("q", step))
             normed_copy(from_plane(step)).wait_send()
@@ -584,11 +667,15 @@
 
 
 COMPUTE = True
-SENDS = (
-    {"k": "k1", "v": "v1 k3 v3 k2 v2", "q": "q1", "f": "q2 q3"},
-    {"k": "k1 k2", "v": "v1 v2 k3 v3", "q": "q1 q2 q3"},
-    {"k": "k1 k3", "v": "v1 v3 k2 v2", "q": "q1 q3 q2"},
-    {"k": "k1", "v": "v1", "q": "q1", "d": "k3 v3 k2 v2 q3 q2"},
+ORDER = (
+    {"k": "k1", "v": "v1k2v2k3v3", "q": "q1", "0": "r0z1w0", "1": "z2r1w1q2q3a1", "2": "z3r2a2", "2b": "w2r3", "3": "a3", "4": "w3"},
+    {"k": "k0", "v": "v0k1v1k2v2k3v3", "q": "q0q1", "0": "z0z1r0w0a0", "1": "z2r1w1q2q3a1", "2": "z3r2a2", "2b": "w2r3", "3": "a3", "4": "w3"},
+    {"k": "k1k2", "v": "v1v2k3v3", "q": "q1q2q3", "0": "r0z1w0", "1": "z2r1z3w1a1", "2": "r2a2", "2b": "w2r3", "3": "a3", "4": "w3"},
+    {"k": "k0", "v": "v0k1v1k2v2k3v3", "q": "q0q1q2q3", "0": "z0z1r0w0a0", "1": "z2r1z3w1a1", "2": "r2a2", "2b": "w2r3", "3": "a3", "4": "w3"},
+    {"k": "k1k2", "v": "v1v2k3v3", "q": "q1q2q3", "0": "r0z1w0", "1": "z2r1z3w1a1", "2": "r2w2", "2b": "r3a2", "3": "a3", "4": "w3"},
+    {"k": "k0", "v": "v0k1v1k2v2k3v3", "q": "q0q1q2q3", "0": "z0z1r0w0a0", "1": "z2r1z3w1a1", "2": "r2w2", "2b": "r3a2", "3": "a3", "4": "w3"},
+    {"k": "k1", "v": "v1k2v2k3v3", "q": "q1", "0": "r0z1w0", "1": "z2r1w1q2q3a1", "2": "z3r2w2", "2b": "r3a2", "3": "a3", "4": "w3"},
+    {"k": "k0", "v": "v0k1v1k2v2k3v3", "q": "q0q1", "0": "z0z1r0w0a0", "1": "z2r1w1q2q3a1", "2": "z3r2w2", "2b": "r3a2", "3": "a3", "4": "w3"},
 )
 
 
@@ -626,6 +713,7 @@
             pltpu.VMEM(value_proj.shape, bf16),
             pltpu.VMEM((2,) + out_proj.shape, bf16),
             pltpu.SMEM(lambdas.shape, jnp.float32),
+            pltpu.VMEM((2, groups, 8, head_v), jnp.float32),
             pltpu.VMEM((1, head_v), jnp.float32),
             pltpu.VMEM((groups, rows, width), bf16),
             pltpu.VMEM((groups, rows, head_v), bf16),
@@ -638,7 +726,10 @@
             pltpu.VMEM((groups, rows // ROW_TILE, 2 * ROW_TILE, LANES), jnp.float32),
             pltpu.VMEM((groups, rows // ROW_TILE, 2 * ROW_TILE, LANES), jnp.float32),
             pltpu.VMEM((groups, rows // ROW_TILE, 2 * ROW_TILE, head_v), jnp.float32),
+            pltpu.VMEM((rows, columns), jnp.float32),
             dma((9,)),
+            dma,
+            dma,
             dma,
             dma,
         ]

time: 39.7 us -> 36.5 us (0.919); the launches traced: 39.6 us -> 35.9 us
  Pallas kernels: 38.6 us -> 34.9 us
    pallas_call x1, Pallas kernels: 38.6 us -> 34.9 us  [fused_shards(): pl.pallas_call(body, name='fused_attention', out_shape=jax.ShapeDtypeStru...]
where the time goes in v4:
time: 36.5 us; the launch traced here: 35.9 us
  Pallas kernels  34.9 us (96%)
  local copies, waits for them, and re-layouts  0.97 us (3%)
    pallas_call x1, Pallas kernels, fused_shards(): pl.pallas_call(body, name='fused_attention', out_shape=jax.ShapeDtypeStru...  34.9 us
    unnamed x1, local copies, waits for them, and re-layouts  0.97 us

profile of v4, /device:TPU:17, one launch (start us, length us, event | category | flops | bytes accessed | tf_op | source)
XLA Modules:
  0.0 35.9 jit_solution(2854092275447219448)
XLA Ops:
  0.0 34.9 %fused_attention.1 = bf16[256,2048]{1,0:T(8,128)(2,1)S(1)} custom-call(bf16[256,2048]{1,0:T(8,128)(2,1)} %refs_0_.1, bf16[2048,256]{1,0:T(8,128)(2,1)} %refs_1_.1, bf16[2048,256]{1,0:T(8,128)(2,1)} %refs_2_.1, bf16[2048,256]{1,0:T(8,128)(2,1)} %refs_3_.1, bf16[2048,256]{1,0:T(8,128)(2,1)} %refs_4_.1, bf16[2048,512]{1,0:T(8,128)(2,1)} %refs_5_.1, f32[4]{0:T(128)} %refs_6_.1, ...), custom_call_target="tpu_custom_call" | custom-call | tf_op jit(solution)/shard_map/fused_attention/pallas_call | solution.py:701
  34.9 1.0 %copy.11 = bf16[256,2048]{1,0:T(8,128)(2,1)} copy(bf16[256,2048]{1,0:T(8,128)(2,1)S(1)} %fused_attention.1) | data formatting | bytes 2097152

commit v5 on v4

--- a/solution.py
+++ b/solution.py
@@ -155,31 +155,18 @@
     acc_all,
     out_acc,
     load_sem,
-    wo_send,
+    sent,
+    wo_sent,
     wo_recv,
-    lam_send,
+    lam_sent,
     lam_recv,
-    zk_send,
     zk_recv,
-    zv_send,
     zv_recv,
-    q_send,
     q_recv,
-    xk_send,
     xk_recv,
-    xv_send,
     xv_recv,
-    yk_send,
-    yk_recv,
-    yv_send,
-    yv_recv,
-    fk_send,
-    fk_recv,
-    fv_send,
-    fv_recv,
-    n_send,
+    y_recv,
     n_recv,
-    r_send,
     r_recv,
 ):
     scope = jax.named_scope
@@ -200,19 +187,30 @@
     def load(index, src, dst):
         return pltpu.make_async_copy(src, dst, load_sem.at[index])
 
-    loads = [
-        load(0, hidden_hbm, hid),
-        load(1, k1_hbm, wk1),
-        load(2, k2_hbm, wk2),
-        load(3, v_hbm, wv),
-        load(4, q1_hbm, wq1),
-        load(5, q2_hbm, wq2),
-        load(6, wo_hbm, wo.at[core]),
-        load(7, lam_hbm, lam_ref),
-        load(8, gain_hbm, gain_ref),
+    depth = hid.shape[1]
+    cut = depth // K_CUTS
+    cuts = [slice(index * cut, (index + 1) * cut) for index in range(K_CUTS)]
+    loads = []
+    for index, part in enumerate(cuts):
+        loads += [
+            load(index, hidden_hbm.at[:, part], hid.at[:, part]),
+            load(index, k1_hbm.at[part], wk1.at[part]),
+            load(index, k2_hbm.at[part], wk2.at[part]),
+        ]
+    loads += [
+        load(K_CUTS, v_hbm, wv),
+        load(K_CUTS + 1, q1_hbm, wq1),
+        load(K_CUTS + 1, q2_hbm, wq2),
+        load(K_CUTS + 2, wo_hbm, wo.at[core]),
+        load(K_CUTS + 3, lam_hbm, lam_ref),
+        load(K_CUTS + 4, gain_hbm, gain_ref),
     ]
     for item in loads:
         item.start()
+
+    def loaded(index, ref):
+        pltpu.make_async_copy(ref, ref, load_sem.at[index]).wait()
+
     barrier = pltpu.get_barrier_semaphore()
 
     def greet(index, tp_index):
@@ -227,11 +225,11 @@
     greet(me, 1 - core)
     greet(me + 1 - 2 * x, core)
 
-    def send(src, dst, send_sem, recv_sem, index, tp_index):
+    def send(src, dst, recv_sem, index, tp_index, send_sem=None):
         return pltpu.make_async_remote_copy(
             src_ref=src,
             dst_ref=dst,
-            send_sem=send_sem,
+            send_sem=sent if send_sem is None else send_sem,
             recv_sem=recv_sem,
             device_id=(index, tp_index),
             device_id_type=MESH,
@@ -261,15 +259,14 @@
 
     def z_copy(kind, step):
         target = from_plane(step)
-        out, full, sems, recvs = {
-            "k": (k_out, k_all.at[me], zk_send, zk_recv),
-            "v": (v_out, v_all.at[me], zv_send, zv_recv),
-            "q": (q_out, q_all.at[plane], q_send, q_recv),
+        out, full, recvs = {
+            "k": (k_out, k_all.at[me], zk_recv),
+            "v": (v_out, v_all.at[me], zv_recv),
+            "q": (q_out, q_all.at[plane], q_recv),
         }[kind]
         return send(
             out.at[target],
             full,
-            sems.at[step],
             recvs.at[plane],
             *owner(target),
         )
@@ -277,10 +274,6 @@
     def z_start(*items):
         for kind, step in items:
             z_copy(kind, step).start()
-
-    def z_done(*items):
-        for kind, step in items:
-            z_copy(kind, step).wait_send()
 
     def perform(items):
         for item in items:
@@ -313,25 +306,25 @@
     def y_block(step):
         return from_plane(step) * PLANE + mine + 2 - 4 * core
 
-    def to_x(slot, sems, recvs, step):
-        return send(slot, slot, sems.at[step], recvs.at[step], me + 1 - 2 * x, core)
-
-    def to_y(slot, sems, recvs, step):
-        return send(slot, slot, sems.at[step], recvs.at[step], me, 1 - core)
+    def to_x(slot, recvs, step):
+        return send(slot, slot, recvs.at[step], me + 1 - 2 * x, core)
+
+    def to_y(slot, step):
+        return send(slot, slot, y_recv.at[step], me, 1 - core)
 
     def spread_k(step):
         slot = k_all.at[from_plane(step) * PLANE + mine]
-        return (to_x(slot, xk_send, xk_recv, step), to_y(slot, yk_send, yk_recv, step))
+        return (to_x(slot, xk_recv, step), to_y(slot, step))
 
     def spread_v(step):
         slot = v_all.at[from_plane(step) * PLANE + mine]
-        return (to_x(slot, xv_send, xv_recv, step), to_y(slot, yv_send, yv_recv, step))
+        return (to_x(slot, xv_recv, step), to_y(slot, step))
 
     def relay_k(step):
-        return (to_y(k_all.at[x_block(step)], fk_send, fk_recv, step),)
+        return (to_y(k_all.at[x_block(step)], step),)
 
     def relay_v(step):
-        return (to_y(v_all.at[x_block(step)], fv_send, fv_recv, step),)
+        return (to_y(v_all.at[x_block(step)], step),)
 
     def start(copies):
         for copy in copies:
@@ -355,26 +348,27 @@
         start(relay_v(step))
 
     def ready(step):
-        far = from_plane(step) * PLANE + (PLANE - 1 - mine)
         with scope(f"ready#s={step}"):
-            arrived(k_all.at[y_block(step)], yk_recv.at[step])
-            arrived(v_all.at[y_block(step)], yv_recv.at[step])
-            arrived(k_all.at[far], fk_recv.at[step])
-            arrived(v_all.at[far], fv_recv.at[step])
+            arrived(k_all.at[pl.ds(0, 4)], y_recv.at[step])
 
     def ready_q(step):
         with scope(f"q#s={step}"):
             slot = q_all.at[from_plane(step)]
             arrived(slot, q_recv.at[from_plane(step)])
 
-    with scope("w_hid"):
-        loads[0].wait()
-    with scope("w_k"):
-        loads[1].wait()
-        loads[2].wait()
     with scope("p_k"):
-        first = project(wk1).astype(jnp.bfloat16)
-        second = project(wk2).astype(jnp.bfloat16)
+        first = second = None
+        for index, part in enumerate(cuts):
+            with scope(f"w_k#{index}"):
+                loaded(index, wv.at[pl.ds(0, cut * (rows + 2 * wk1.shape[1]) // wv.shape[1])])
+            more = [
+                jnp.dot(hid[:, part], weight[part], preferred_element_type=jnp.float32)
+                for weight in (wk1, wk2)
+            ]
+            first = more[0] if first is None else first + more[0]
+            second = more[1] if second is None else second + more[1]
+        first = first.astype(jnp.bfloat16)
+        second = second.astype(jnp.bfloat16)
 
         def put_k(head, value):
             k_out[head] = value
@@ -390,7 +384,7 @@
     pl.when(home)(lambda: start(spread_k(0)))
     moment("k")
     with scope("w_v"):
-        loads[3].wait()
+        loaded(K_CUTS, wv)
     with scope("p_v"):
         value = project(wv).astype(jnp.bfloat16)
         for head in range(groups):
@@ -403,8 +397,7 @@
     pl.when(home)(lambda: start(spread_v(0)))
     moment("v")
     with scope("w_q"):
-        loads[4].wait()
-        loads[5].wait()
+        loaded(K_CUTS + 1, wv)
     with scope("p_q"):
         first = (project(wq1) * score_scale).astype(jnp.bfloat16)
         second = (project(wq2) * score_scale).astype(jnp.bfloat16)
@@ -419,14 +412,14 @@
             q_all[plane] = q_out[plane]
 
     moment("q")
-    loads[6].wait()
-    wo_copy = send(wo.at[core], wo.at[core], wo_send, wo_recv, me, 1 - core)
+    loaded(K_CUTS + 2, wo.at[core])
+    wo_copy = send(wo.at[core], wo.at[core], wo_recv, me, 1 - core, wo_sent)
     wo_copy.start()
-    loads[7].wait()
-    loads[8].wait()
+    loads[-2].wait()
+    loads[-1].wait()
     for head in range(groups):
         lam_all[core, head] = jnp.full(lam_all.shape[2:], lam_ref[head], jnp.float32)
-    lam_copy = send(lam_all.at[core], lam_all.at[core], lam_send, lam_recv, me, 1 - core)
+    lam_copy = send(lam_all.at[core], lam_all.at[core], lam_recv, me, 1 - core, lam_sent)
     lam_copy.start()
 
     tile = ROW_TILE
@@ -494,14 +487,13 @@
         return send(
             n_out.at[group],
             n_all.at[y, plane],
-            n_send.at[group],
             n_recv.at[plane],
             *owner(group),
         )
 
     def partner_copy(head):
         slot = n_all.at[core, head]
-        return send(slot, slot, r_send.at[head], r_recv.at[head], me, 1 - core)
+        return send(slot, slot, r_recv.at[head // half], me, 1 - core)
 
     gain = gain_ref[...]
 
@@ -642,30 +634,22 @@
     arrived(wo.at[1 - core], wo_recv)
     for first in range(0, groups, half):
         with scope(f"rrecv#f={first}"):
-            for head in range(first, first + half):
-                arrived(n_all.at[1 - core, head], r_recv.at[head])
+            arrived(n_all.at[1 - core, pl.ds(first, half)], r_recv.at[first // half])
         out_part(1 - core, first, first + half == groups)
 
     with scope("drain"):
         wo_copy.wait_send()
         lam_copy.wait_send()
-        for step in range(groups):
-            for copies in (spread_k, spread_v, relay_k, relay_v):
-                for copy in copies(step):
-                    copy.wait_send()
-
-        @pl.when(away)
-        def _():
-            z_done(("k", 0), ("v", 0), ("q", 0))
-            normed_copy(plane).wait_send()
-
-        for step in range(1, groups):
-            z_done(("k", step), ("v", step), ("q", step))
-            normed_copy(from_plane(step)).wait_send()
-        for head in range(groups):
-            partner_copy(head).wait_send()
-
-
+        unit = rows * width // (2 * wo.shape[2])
+        for place, extra in ((home, 0), (away, 4)):
+            blocks = (groups - 1) * 4 + 6 * groups + groups + extra
+
+            @pl.when(place)
+            def _():
+                arrived(wo.at[:, pl.ds(0, blocks * unit)], sent)
+
+
+K_CUTS = 4
 COMPUTE = True
 ORDER = (
     {"k": "k1", "v": "v1k2v2k3v3", "q": "q1", "0": "r0z1w0", "1": "z2r1w1q2q3a1", "2": "z3r2a2", "2b": "w2r3", "3": "a3", "4": "w3"},
@@ -727,13 +711,15 @@
             pltpu.VMEM((groups, rows // ROW_TILE, 2 * ROW_TILE, LANES), jnp.float32),
             pltpu.VMEM((groups, rows // ROW_TILE, 2 * ROW_TILE, head_v), jnp.float32),
             pltpu.VMEM((rows, columns), jnp.float32),
-            dma((9,)),
+            dma((K_CUTS + 5,)),
+            dma,
             dma,
             dma,
             dma,
             dma,
         ]
-        + [dma((groups,))] * 22,
+        + [dma((groups,))] * 7
+        + [dma((2,))],
         compiler_params=pltpu.CompilerParams(
             collective_id=0, has_side_effects=True, vmem_limit_bytes=VMEM_LIMIT
         ),

time: 36.5 us -> 35.7 us (0.978)
  Pallas kernels: 34.9 us -> 34.1 us
    pallas_call x1, Pallas kernels: 34.9 us -> 34.1 us  [fused_shards(): pl.pallas_call(body, name='fused_attention', out_shape=jax.ShapeDtypeStru...]
where the time goes in v5:
time: 35.7 us; the launch traced here: 35.1 us
  Pallas kernels  34.1 us (96%)
  local copies, waits for them, and re-layouts  0.97 us (3%)
    pallas_call x1, Pallas kernels, fused_shards(): pl.pallas_call(body, name='fused_attention', out_shape=jax.ShapeDtypeStru...  34.1 us
    unnamed x1, local copies, waits for them, and re-layouts  0.97 us

profile of v5, /device:TPU:17, one launch (start us, length us, event | category | flops | bytes accessed | tf_op | source)
XLA Modules:
  0.0 35.1 jit_solution(14657220121047453344)
XLA Ops:
  0.0 34.1 %fused_attention.1 = bf16[256,2048]{1,0:T(8,128)(2,1)S(1)} custom-call(bf16[256,2048]{1,0:T(8,128)(2,1)} %refs_0_.1, bf16[2048,256]{1,0:T(8,128)(2,1)} %refs_1_.1, bf16[2048,256]{1,0:T(8,128)(2,1)} %refs_2_.1, bf16[2048,256]{1,0:T(8,128)(2,1)} %refs_3_.1, bf16[2048,256]{1,0:T(8,128)(2,1)} %refs_4_.1, bf16[2048,512]{1,0:T(8,128)(2,1)} %refs_5_.1, f32[4]{0:T(128)} %refs_6_.1, ...), custom_call_target="tpu_custom_call" | custom-call | tf_op jit(solution)/shard_map/fused_attention/pallas_call | solution.py:685
  34.1 1.0 %copy.11 = bf16[256,2048]{1,0:T(8,128)(2,1)} copy(bf16[256,2048]{1,0:T(8,128)(2,1)S(1)} %fused_attention.1) | data formatting | bytes 2097152

commit v6 on v5

--- a/solution.py
+++ b/solution.py
@@ -424,18 +424,18 @@
 
     tile = ROW_TILE
     tiles = rows // tile
-    chunk = PLANE * rows
     lane = lax.broadcasted_iota(jnp.int32, (tile, width), 1)
 
-    def pair_tile(group, key_group, part, diagonal):
+    def pair_tile(group, key_group, part, diagonal, span):
+        chunk = span * rows
         begin_row = pl.multiple_of(part * tile, tile)
         queries = q_all[group, pl.ds(begin_row, tile), :]
         zero = jnp.zeros_like(queries)
         both = jnp.concatenate(
             (jnp.where(lane < qk, queries, zero), jnp.where(lane >= qk, queries, zero)), axis=0
         )
-        keys = k_all[pl.ds(key_group * PLANE, PLANE)].reshape(chunk, width)
-        values = v_all[pl.ds(key_group * PLANE, PLANE)].reshape(chunk, head_v)
+        keys = k_all[pl.ds(key_group * PLANE, span)].reshape(chunk, width)
+        values = v_all[pl.ds(key_group * PLANE, span)].reshape(chunk, head_v)
         scores = lax.dot_general(
             both, keys, (((1,), (1,)), ((), ())), preferred_element_type=jnp.float32
         )
@@ -471,12 +471,12 @@
         sum_all[group, part] = sum_all[group, part] * rescale + new_sum
         acc_all[group, part] = acc_all[group, part] * rescale + accum
 
-    def pair(group, key_group, diagonal):
+    def pair(group, key_group, diagonal, span=PLANE):
         if not COMPUTE:
             return
         with scope("pair_d" if diagonal else "pair"):
             lax.fori_loop(
-                0, tiles, lambda t, c: (pair_tile(group, key_group, t, diagonal), c)[1], 0
+                0, tiles, lambda t, c: (pair_tile(group, key_group, t, diagonal, span), c)[1], 0
             )
 
     def meet(step, earlier):
@@ -537,7 +537,9 @@
     acc_all[...] = jnp.zeros(acc_all.shape, jnp.float32)
 
     def diagonal(step):
-        pair(from_plane(step), from_plane(step), True)
+        group = from_plane(step)
+        pl.when(core == 0)(lambda: pair(group, group, True, PLANE // 2))
+        pl.when(core != 0)(lambda: pair(group, group, True))
 
     moment("0")
     arrived(lam_all.at[1 - core], lam_recv)

time: 35.7 us -> 35.2 us (0.986)
  no operation moved by 1% of the time
where the time goes in v6:
time: 35.2 us; the launch traced here: 34.8 us
  Pallas kernels  33.8 us (96%)
  local copies, waits for them, and re-layouts  0.97 us (3%)
    pallas_call x1, Pallas kernels, fused_shards(): pl.pallas_call(body, name='fused_attention', out_shape=jax.ShapeDtypeStru...  33.8 us
    unnamed x1, local copies, waits for them, and re-layouts  0.97 us

profile of v6, /device:TPU:17, one launch (start us, length us, event | category | flops | bytes accessed | tf_op | source)
XLA Modules:
  0.0 34.8 jit_solution(7842452372652623918)
XLA Ops:
  0.0 33.8 %fused_attention.1 = bf16[256,2048]{1,0:T(8,128)(2,1)S(1)} custom-call(bf16[256,2048]{1,0:T(8,128)(2,1)} %refs_0_.1, bf16[2048,256]{1,0:T(8,128)(2,1)} %refs_1_.1, bf16[2048,256]{1,0:T(8,128)(2,1)} %refs_2_.1, bf16[2048,256]{1,0:T(8,128)(2,1)} %refs_3_.1, bf16[2048,256]{1,0:T(8,128)(2,1)} %refs_4_.1, bf16[2048,512]{1,0:T(8,128)(2,1)} %refs_5_.1, f32[4]{0:T(128)} %refs_6_.1, ...), custom_call_target="tpu_custom_call" | custom-call | tf_op jit(solution)/shard_map/fused_attention/pallas_call | solution.py:687
  33.8 1.0 %copy.11 = bf16[256,2048]{1,0:T(8,128)(2,1)} copy(bf16[256,2048]{1,0:T(8,128)(2,1)S(1)} %fused_attention.1) | data formatting | bytes 2097152

commit v7 on v6

--- a/solution.py
+++ b/solution.py
@@ -538,8 +538,8 @@
 
     def diagonal(step):
         group = from_plane(step)
-        pl.when(core == 0)(lambda: pair(group, group, True, PLANE // 2))
-        pl.when(core != 0)(lambda: pair(group, group, True))
+        for last in range(PLANE):
+            pl.when(mine == last)(lambda last=last: pair(group, group, True, last + 1))
 
     moment("0")
     arrived(lam_all.at[1 - core], lam_recv)

time: 35.2 us -> 35.4 us (level)
  no operation moved by 1% of the time
where the time goes in v7:
time: 35.4 us; the launch traced here: 34.8 us
  Pallas kernels  33.8 us (95%)
  local copies, waits for them, and re-layouts  0.97 us (3%)
    pallas_call x1, Pallas kernels, fused_shards(): pl.pallas_call(body, name='fused_attention', out_shape=jax.ShapeDtypeStru...  33.8 us
    unnamed x1, local copies, waits for them, and re-layouts  0.97 us

profile of v7, /device:TPU:17, one launch (start us, length us, event | category | flops | bytes accessed | tf_op | source)
XLA Modules:
  0.0 34.8 jit_solution(1654403047518659399)
XLA Ops:
  0.0 33.8 %fused_attention.1 = bf16[256,2048]{1,0:T(8,128)(2,1)S(1)} custom-call(bf16[256,2048]{1,0:T(8,128)(2,1)} %refs_0_.1, bf16[2048,256]{1,0:T(8,128)(2,1)} %refs_1_.1, bf16[2048,256]{1,0:T(8,128)(2,1)} %refs_2_.1, bf16[2048,256]{1,0:T(8,128)(2,1)} %refs_3_.1, bf16[2048,256]{1,0:T(8,128)(2,1)} %refs_4_.1, bf16[2048,512]{1,0:T(8,128)(2,1)} %refs_5_.1, f32[4]{0:T(128)} %refs_6_.1, ...), custom_call_target="tpu_custom_call" | custom-call | tf_op jit(solution)/shard_map/fused_attention/pallas_call | solution.py:687
  33.9 1.0 %copy.11 = bf16[256,2048]{1,0:T(8,128)(2,1)} copy(bf16[256,2048]{1,0:T(8,128)(2,1)S(1)} %fused_attention.1) | data formatting | bytes 2097152
